TPU v7x, 128 devices: a whole 4x4x4 slice. The times are simulated.
128 devices in a mesh: sp: 32 (over z, y, core), tp: 4 (over x).
Axes of the slice: x: 4, y: 4, z: 4, core: 2. Of those that a mesh axis runs over, the one named last changes fastest.
Arguments:
- expert_input: bfloat16 [12288, 2048], P('sp'), may hold values from -6 to 6
- cotangent: bfloat16 [12288, 2048], P('sp'), may hold values from -6 to 6
- routes: int32 [12288, 2], P('sp'), may hold values from 0 to 31, all different within a row; in each aligned block of 384 rows (0 to 383, 384 to 767, ...) at most 36 rows name the same one
- route_weight: float32 [12288, 2], P('sp'), may hold values from 0.2 to 2.5
- expert_gate: bfloat16 [32, 2048, 1024], P('sp', None, 'tp'), may hold values from -0.125 to 0.125
- expert_up: bfloat16 [32, 2048, 1024], P('sp', None, 'tp'), may hold values from -0.125 to 0.125
- expert_down: bfloat16 [32, 1024, 2048], P('sp', 'tp'), may hold values from -0.1875 to 0.1875
- conv_out: bfloat16 [12288, 1024], P('sp', 'tp'), may hold values from -14 to 14
- conv_value: bfloat16 [12288, 1024], P('sp', 'tp'), may hold values from -6 to 6
- conv_gate: bfloat16 [12288, 1024], P('sp', 'tp'), may hold values from -6 to 6
- conv_taps: float32 [31, 1024], P(None, 'tp'), may hold values from -1 to 1
- norm_gain: float32 [1024], P('tp'), may hold values from 0.1 to 1.9
- norm_bias: float32 [1024], P('tp'), may hold values from -3 to 3
- out_weight: bfloat16 [1024, 2048], P('tp'), may hold values from -0.1875 to 0.1875
Outputs:
- gate_grad: float32 [32, 2048, 1024], P('sp', None, 'tp')
- up_grad: float32 [32, 2048, 1024], P('sp', None, 'tp')
- down_grad: float32 [32, 1024, 2048], P('sp', 'tp')
- resid_grad: bfloat16 [12288, 2048], P('sp')
- out_weight_grad: float32 [1024, 2048], P('tp', 'sp')
- value_grad: bfloat16 [12288, 1024], P('sp', 'tp')
- gate_in_grad: bfloat16 [12288, 1024], P('sp', 'tp')
Inputs may be any that keep to these rules, and one draw needn't show every extreme that they name: `routes`: each token names 2 different experts. In each aligned block of 384 tokens no expert is named by more than 36 tokens, and in every draw some block has an expert named by exactly 36 tokens.
All inputs are finite; a program needn't handle non-finite values.
Results may differ from a plain program's by a relative error of at most 0.018.
Values may be sent and summed in bfloat16 or wider, within the bound.
A program may use at most 128 MiB of HBM per device.

v0:
```python
import jax
import jax.numpy as jnp
from jax import lax
from jax.sharding import PartitionSpec as P

norm_eps = 1e-06


def passed_along(value, axis, steps):
    count = lax.axis_size(axis)
    leading, last = (max(0, -steps), min(count, count - steps))
    return lax.ppermute(value, axis, [(source, source + steps) for source in range(leading, last)])


def cut_along(x, dim, size):
    lengths = x.shape
    tiles = x.reshape(*lengths[:dim], size, lengths[dim] // size, *lengths[dim + 1 :])
    return jnp.moveaxis(tiles, dim, 0)


def sent_and_summed(x, axis, dim):
    size = lax.axis_size(axis)
    tiles = lax.all_to_all(cut_along(x, dim, size), axis, 0, 0, tiled=True)
    return jnp.sum(tiles.astype(jnp.float32), axis=0)


def on_device(
    expert_input,
    cotangent,
    routes,
    route_weight,
    expert_gate,
    expert_up,
    expert_down,
    conv_out,
    conv_value,
    conv_gate,
    conv_taps,
    norm_gain,
    norm_bias,
    out_weight,
):
    sp_count = lax.axis_size("sp")
    tp_count = lax.axis_size("tp")
    tok_rows, model_width = expert_input.shape
    share_cols = model_width // tp_count
    top_count = routes.shape[1]
    local_exp = expert_gate.shape[0]
    experts = local_exp * sp_count
    capacity = 3 * top_count * tok_rows // (2 * experts)
    assigns = tok_rows * top_count
    flat_routes = routes.reshape(assigns)
    onehot = (flat_routes[:, None] == jnp.arange(experts, dtype=jnp.int32)[None, :]).astype(
        jnp.int32
    )
    slot_rank = jnp.sum((jnp.cumsum(onehot, axis=0) - onehot) * onehot, axis=1)
    target = flat_routes * capacity + slot_rank
    slot_ids = (
        jnp.full((experts * capacity,), assigns, jnp.int32)
        .at[target]
        .set(jnp.arange(assigns, dtype=jnp.int32))
    )
    token_of = slot_ids // top_count
    padded_in = jnp.concatenate([expert_input, jnp.zeros((1, model_width), jnp.bfloat16)], axis=0)
    padded_cot = jnp.concatenate([cotangent, jnp.zeros((1, model_width), jnp.bfloat16)], axis=0)
    padded_weight = jnp.concatenate(
        [route_weight.reshape(assigns), jnp.zeros((1,), jnp.float32)], axis=0
    )
    send_rows = padded_in[token_of].reshape(experts, capacity, model_width)
    send_cot = (padded_cot[token_of].astype(jnp.float32) * padded_weight[slot_ids][:, None]).astype(
        jnp.bfloat16
    )
    send_cot = send_cot.reshape(experts, capacity, model_width)
    got_rows, got_cot = (
        lax.all_to_all(send_rows, "sp", split_axis=0, concat_axis=0, tiled=True),
        lax.all_to_all(send_cot, "sp", split_axis=0, concat_axis=0, tiled=True),
    )

    def by_expert(arrived):
        return (
            arrived.reshape(sp_count, local_exp, capacity, model_width)
            .transpose(1, 0, 2, 3)
            .reshape(local_exp, sp_count * capacity, model_width)
        )

    slot_rows = by_expert(got_rows)
    slot_cots = by_expert(got_cot)
    pre_gate = jnp.einsum(
        "lrd,ldf->lrf", slot_rows, expert_gate, preferred_element_type=jnp.float32
    )
    pre_up = jnp.einsum("lrd,ldf->lrf", slot_rows, expert_up, preferred_element_type=jnp.float32)
    gate_sig = jax.nn.sigmoid(pre_gate)
    gate_act = pre_gate * gate_sig
    hidden = (gate_act * pre_up).astype(jnp.bfloat16)
    hidden_grad = jnp.einsum(
        "lrd,lfd->lrf", slot_cots, expert_down, preferred_element_type=jnp.float32
    )
    down_grad = jnp.einsum("lrf,lrd->lfd", hidden, slot_cots, preferred_element_type=jnp.float32)
    gate_pre = (hidden_grad * pre_up * gate_sig * (1.0 + pre_gate * (1.0 - gate_sig))).astype(
        jnp.bfloat16
    )
    up_pre = (hidden_grad * gate_act).astype(jnp.bfloat16)
    gate_grad = jnp.einsum("lrd,lrf->ldf", slot_rows, gate_pre, preferred_element_type=jnp.float32)
    up_grad = jnp.einsum("lrd,lrf->ldf", slot_rows, up_pre, preferred_element_type=jnp.float32)
    partial_rows = jnp.einsum(
        "lrf,ldf->lrd", gate_pre, expert_gate, preferred_element_type=jnp.float32
    )
    partial_rows = partial_rows + jnp.einsum(
        "lrf,ldf->lrd", up_pre, expert_up, preferred_element_type=jnp.float32
    )
    partial_src = (
        partial_rows.reshape(local_exp, sp_count, capacity, model_width)
        .transpose(1, 0, 2, 3)
        .reshape(experts, capacity, model_width)
    )
    partial_low = partial_src.astype(jnp.bfloat16)
    row_share = lax.psum_scatter(partial_low, "tp", scatter_dimension=2, tiled=True).astype(
        jnp.float32
    )
    slot_back = lax.all_to_all(
        row_share.astype(jnp.bfloat16), "sp", split_axis=0, concat_axis=0, tiled=True
    )
    picked = slot_back.reshape(experts * capacity, share_cols)[target].astype(jnp.float32)
    combined = jnp.sum(picked.reshape(tok_rows, top_count, share_cols), axis=1)
    own_cot = lax.dynamic_slice_in_dim(cotangent, lax.axis_index("tp") * share_cols, share_cols, 1)
    resid_part = (own_cot.astype(jnp.float32) + combined).astype(jnp.bfloat16)
    resid_grad = lax.all_gather(resid_part, "tp", axis=1, tiled=True)
    mix_grad = lax.dot_general(
        resid_grad, out_weight, (((1,), (1,)), ((), ())), preferred_element_type=jnp.float32
    )
    channels = conv_out.shape[1] * tp_count
    conv_vals = conv_out.astype(jnp.float32)
    row_sum, row_square = lax.psum(
        (jnp.sum(conv_vals, axis=1), jnp.sum(conv_vals * conv_vals, axis=1)), "tp"
    )
    row_mean = (row_sum / channels)[:, None]
    row_var = (row_square / channels)[:, None] - row_mean * row_mean
    row_rstd = lax.rsqrt(row_var + norm_eps)
    normed = (conv_vals - row_mean) * row_rstd
    norm_pre = normed * norm_gain[None, :] + norm_bias[None, :]
    norm_sig = jax.nn.sigmoid(norm_pre)
    conv_act = (norm_pre * norm_sig).astype(jnp.bfloat16)
    norm_grad = mix_grad * norm_sig * (1.0 + norm_pre * (1.0 - norm_sig)) * norm_gain[None, :]
    grad_sum, grad_dot = lax.psum(
        (jnp.sum(norm_grad, axis=1), jnp.sum(norm_grad * normed, axis=1)), "tp"
    )
    conv_grad = row_rstd * (
        norm_grad - (grad_sum / channels)[:, None] - normed * (grad_dot / channels)[:, None]
    )
    taps_count = conv_taps.shape[0]
    next_rows = passed_along(conv_grad[: taps_count - 1], "sp", -1)
    extended = jnp.concatenate([conv_grad, next_rows], axis=0)
    glu_grad = jnp.zeros_like(conv_grad)
    for lag_index in range(taps_count):
        begin = taps_count - 1 - lag_index
        glu_grad = glu_grad + conv_taps[lag_index][None, :] * extended[begin : begin + tok_rows]
    gate_sig_in = jax.nn.sigmoid(conv_gate.astype(jnp.float32))
    value_grad = (glu_grad * gate_sig_in).astype(jnp.bfloat16)
    gate_in_grad = (
        glu_grad * conv_value.astype(jnp.float32) * gate_sig_in * (1.0 - gate_sig_in)
    ).astype(jnp.bfloat16)
    projected = sent_and_summed(
        lax.dot_general(
            resid_grad, conv_act, (((0,), (0,)), ((), ())), preferred_element_type=jnp.float32
        ).astype(jnp.bfloat16),
        "sp",
        0,
    )
    out_weight_grad = projected.T
    return (gate_grad, up_grad, down_grad, resid_grad, out_weight_grad, value_grad, gate_in_grad)


def solution(mesh):
    return jax.shard_map(
        on_device,
        mesh=mesh,
        in_specs=(
            P("sp", None),
            P("sp", None),
            P("sp", None),
            P("sp", None),
            P("sp", None, "tp"),
            P("sp", None, "tp"),
            P("sp", "tp", None),
            P("sp", "tp"),
            P("sp", "tp"),
            P("sp", "tp"),
            P(None, "tp"),
            P("tp"),
            P("tp"),
            P("tp", None),
        ),
        out_specs=(
            P("sp", None, "tp"),
            P("sp", None, "tp"),
            P("sp", "tp", None),
            P("sp", None),
            P("tp", "sp"),
            P("sp", "tp"),
            P("sp", "tp"),
        ),
        check_vma=False,
    )
```

profile of v0, /device:TPU:1, one launch (start us, length us, event | category | flops | bytes accessed | tf_op | source)
XLA Modules:
  0.0 354.5 jit_solution(16457883766976699686)
XLA Ops:
  7.2 0.0 copy-start
  7.2 0.8 broadcast_multiply_fusion
  8.0 0.8 copy.22
  8.8 0.1 eq.25
  8.9 0.1 eq.29
  9.1 0.1 copy.21
  9.2 0.2 mul.443
  9.4 1.7 reduce-window.6
  11.1 0.3 slice_reduce_fusion
  11.4 0.1 fusion.128
  11.6 3.4 scatter_custom_fusion
  15.0 1.5 concatenate.12
  16.5 5.9 %gather_fusion = bf16[1152,2048]{1,0:T(8,128)(2,1)} fusion(bf16[385,2048]{1,0:T(8,128)(2,1)S(1)} %concatenate.12, s32[2048]{0:T(1024)S(1)} %get-tuple-element.56), kind=kCustom, calls=%fused_computation | custom fusion | bytes 9441792 | tf_op jit(solution)/shard_map/gather | solution.py:69
  22.5 7.2 %reshape.161 = bf16[32,36,2048]{2,1,0:T(8,128)(2,1)} reshape(bf16[1152,2048]{1,0:T(8,128)(2,1)} %gather_fusion) | data formatting | bytes 9437184 | tf_op jit(solution)/shard_map/reshape | solution.py:69
  29.7 9.6 %all-to-all-start = ((bf16[32,36,2048]{2,1,0:T(8,128)(2,1)}), bf16[32,36,2048]{2,1,0:T(8,128)(2,1)}, u32[]{:S(2)}, u32[]{:S(2)}) async-start(bf16[32,36,2048]{2,1,0:T(8,128)(2,1)} %reshape.161), calls=%async_computation | async-start | bytes 10485760 | tf_op jit(solution)/shard_map/all_to_all | solution.py:75
  39.3 1.5 concatenate.13
  40.8 6.0 %gather_fusion.1 = bf16[1152,2048]{1,0:T(8,128)(2,1)} fusion(bf16[385,2048]{1,0:T(8,128)(2,1)S(1)} %concatenate.13, s32[2048]{0:T(1024)S(1)} %get-tuple-element.56), kind=kCustom, calls=%fused_computation.1 | custom fusion | bytes 9441792 | tf_op jit(solution)/shard_map/gather | solution.py:70
  46.8 7.9 %reshape.170 = f32[32,36,2048]{2,1,0:T(8,128)} reshape(bf16[1152,2048]{1,0:T(8,128)(2,1)} %gather_fusion.1) | data formatting | bytes 14155776 | tf_op jit(solution)/shard_map/convert_element_type | solution.py:70
  54.7 0.1 copy.25
  54.8 0.1 reshape.163
  55.0 4.6 %gather_fusion.2 = f32[1152]{0:T(1024)S(1)} fusion(f32[769]{0:T(1024)S(1)} %pad_maximum_fusion.1, s32[2048]{0:T(1024)S(1)} %get-tuple-element.55), kind=kCustom, calls=%fused_computation.2 | custom fusion | bytes 13824 | tf_op jit(solution)/shard_map/gather | solution.py:70
  59.6 0.1 mul.445
  59.7 6.9 %multiply_convert_fusion = bf16[32,36,2048]{2,1,0:T(8,128)(2,1)} fusion(f32[32,36,2048]{2,1,0:T(8,128)} %reshape.170, f32[32,36]{1,0:T(8,128)S(1)} %mul.445), kind=kLoop, calls=%fused_computation.5 | loop fusion | flops 4718592 | bytes 14160384 | tf_op jit(solution)/shard_map/convert_element_type | solution.py:70
  66.6 34.6 %all-to-all-done = bf16[32,36,2048]{2,1,0:T(8,128)(2,1)} async-done(((bf16[32,36,2048]{2,1,0:T(8,128)(2,1)}), bf16[32,36,2048]{2,1,0:T(8,128)(2,1)}, u32[]{:S(2)}, u32[]{:S(2)}) %all-to-all-start) | async-done | bytes 4718624 | tf_op jit(solution)/shard_map/all_to_all | solution.py:75
  101.2 8.8 %all-to-all-start.1 = ((bf16[32,36,2048]{2,1,0:T(8,128)(2,1)}), bf16[32,36,2048]{2,1,0:T(8,128)(2,1)}, u32[]{:S(2)}, u32[]{:S(2)}) async-start(bf16[32,36,2048]{2,1,0:T(8,128)(2,1)} %multiply_convert_fusion), calls=%async_computation.1 | async-start | bytes 10485760 | tf_op jit(solution)/shard_map/all_to_all | solution.py:76
  110.0 0.2 reduce-scatter.2.cloned.1.call-start
  110.2 7.2 %reshape.162 = bf16[1152,2048]{1,0:T(8,128)(2,1)} reshape(bf16[32,36,2048]{2,1,0:T(8,128)(2,1)} %all-to-all-done) | data formatting | bytes 9437184 | tf_op jit(solution)/shard_map/reshape.20
  117.4 4.9 %fusion.6 = f32[1152,256]{1,0:T(8,128)} fusion(bf16[1152,2048]{1,0:T(8,128)(2,1)} %reshape.162, bf16[1,2048,256]{2,1,0:T(8,128)(2,1)S(1)} %copy-done), kind=kOutput, calls=%fused_computation.52 | convolution fusion | flops 1207959552 | bytes 6946816 | tf_op jit(solution)/shard_map/lrd,ldf->lrf/dot_general | solution.py:88
  122.3 2.4 fusion.9
  124.8 47.1 %all-to-all-done.1 = bf16[32,36,2048]{2,1,0:T(8,128)(2,1)} async-done(((bf16[32,36,2048]{2,1,0:T(8,128)(2,1)}), bf16[32,36,2048]{2,1,0:T(8,128)(2,1)}, u32[]{:S(2)}, u32[]{:S(2)}) %all-to-all-start.1) | async-done | bytes 4718624 | tf_op jit(solution)/shard_map/all_to_all | solution.py:76
  171.9 7.2 %reshape.164 = bf16[1152,2048]{1,0:T(8,128)(2,1)} reshape(bf16[32,36,2048]{2,1,0:T(8,128)(2,1)} %all-to-all-done.1) | data formatting | bytes 9437184 | tf_op jit(solution)/shard_map/reshape.3
  179.1 4.7 %multiply_convert_fusion.2 = (bf16[1152,256]{1,0:T(8,128)(2,1)S(1)}, bf16[1152,256]{1,0:T(8,128)(2,1)S(1)}) fusion(f32[1152,256]{1,0:T(8,128)} %fusion.6, f32[1152,256]{1,0:T(8,128)} %fusion.9, bf16[1152,2048]{1,0:T(8,128)(2,1)} %reshape.164, bf16[1,256,2048]{2,1,0:T(8,128)(2,1)S(1)} %copy-done.12), kind=kOutput, calls=%fused_computation.46 | convolution fusion | flops 1211793408 | bytes 9306112 | tf_op jit(solution)/shard_map/lrd,lfd->lrf/dot_general | solution.py:95
  183.8 1.4 fusion.4
  185.3 3.6 %fusion = bf16[1152,2048]{1,0:T(8,128)(2,1)} fusion(f32[1152,2048]{1,0:T(8,128)S(1)} %fusion.4, bf16[1152,256]{1,0:T(8,128)(2,1)S(1)} %get-tuple-element.17, bf16[1,2048,256]{2,1,0:T(8,128)(2,1)S(1)} %copy-done.4), kind=kOutput, calls=%fused_computation.7 | convolution fusion | flops 1212678144 | bytes 15794176 | tf_op jit(solution)/shard_map/lrf,ldf->lrd/dot_general | solution.py:108
  188.8 7.2 %convert_element_type.85 = bf16[32,36,2048]{2,1,0:T(8,128)(2,1)} reshape(bf16[1152,2048]{1,0:T(8,128)(2,1)} %fusion) | data formatting | bytes 9437184 | tf_op jit(solution)/shard_map/convert_element_type | solution.py:116
  196.1 0.0 reduce-scatter.2.cloned.1.call-update
  196.1 55.8 %reduce-scatter.2.cloned.1.call-done = bf16[32,36,512]{2,1,0:T(8,128)(2,1)} async-done(((bf16[32,36,2048]{2,1,0:T(8,128)(2,1)}), bf16[32,36,512]{2,1,0:T(8,128)(2,1)}) %reduce-scatter.2.cloned.1.call-update) | async-done | bytes 1179664 | tf_op jit(solution)/shard_map/reduce_scatter | solution.py:117
  251.9 7.8 %all-to-all-start.2 = ((bf16[32,36,512]{2,1,0:T(8,128)(2,1)}), bf16[32,36,512]{2,1,0:T(8,128)(2,1)S(1)}, u32[]{:S(2)}, u32[]{:S(2)}) async-start(bf16[32,36,512]{2,1,0:T(8,128)(2,1)} %reduce-scatter.2.cloned.1.call-done), calls=%async_computation.3 | async-start | bytes 2621440 | tf_op jit(solution)/shard_map/all_to_all | solution.py:120
  259.6 0.0 all-gather.2.cloned.1.call-start
  259.7 19.2 %all-to-all-done.2 = bf16[32,36,512]{2,1,0:T(8,128)(2,1)S(1)} async-done(((bf16[32,36,512]{2,1,0:T(8,128)(2,1)}), bf16[32,36,512]{2,1,0:T(8,128)(2,1)S(1)}, u32[]{:S(2)}, u32[]{:S(2)}) %all-to-all-start.2) | async-done | bytes 1179680 | tf_op jit(solution)/shard_map/all_to_all | solution.py:120
  278.9 0.2 reshape.168
  279.2 2.7 gather_fusion.3
  281.9 1.0 reshape.171
  282.8 0.0 copy-start.10
  282.8 1.9 reduce_sum.67
  284.8 2.0 add_convert_fusion
  286.7 0.0 all-gather.2.cloned.1.call-update
  286.8 0.2 convert_reduce_fusion.1
  286.9 6.8 %all-reduce.3 = (f32[384]{0:T(512)S(1)}, f32[384]{0:T(512)S(1)}) all-reduce(f32[384]{0:T(512)S(1)} %get-tuple-element.10, f32[384]{0:T(512)S(1)} %get-tuple-element.9), channel_id=1, replica_groups=mesh['sp'=32,'tp'=4] {'tp'}, use_global_device_ids=true, to_apply=%region_9.10 | all-reduce | flops 768 | bytes 6144 | tf_op jit(solution)/shard_map/psum | solution.py:133
  293.8 0.0 copy-start.16
  293.8 5.4 %convolution_bitcast_fusion.2 = f32[1,2048,256]{2,1,0:T(8,128)} fusion(bf16[1152,2048]{1,0:T(8,128)(2,1)} %reshape.162, bf16[1152,256]{1,0:T(8,128)(2,1)S(1)} %copy-done.3), kind=kOutput, calls=%fused_computation.39 | convolution fusion | flops 1207959552 | bytes 7405568 | tf_op jit(solution)/shard_map/lrd,lrf->ldf/dot_general | solution.py:103
  299.3 3.0 convolution_bitcast_fusion
  302.2 7.4 %all-gather.2.cloned.1.call-done = bf16[384,2048]{1,0:T(8,128)(2,1)} async-done(((bf16[384,512]{1,0:T(8,128)(2,1)}), bf16[384,2048]{1,0:T(8,128)(2,1)}) %all-gather.2.cloned.1.call-update) | async-done | bytes 1572880 | tf_op jit(solution)/shard_map/all_gather | solution.py:127
  309.6 3.3 convolution_convert_fusion
  312.9 7.9 %all-to-all-start.3 = ((bf16[32,64,256]{2,1,0:T(8,128)(2,1)}), bf16[32,64,256]{2,1,0:T(8,128)(2,1)S(1)}, u32[]{:S(2)}, u32[]{:S(2)}) async-start(bf16[32,64,256]{2,1,0:T(8,128)(2,1)} %bitcast.7), calls=%async_computation.4 | async-start | bytes 2097152 | tf_op jit(solution)/shard_map/all_to_all | solution.py:23
  320.8 2.5 fusion.137
  323.3 8.0 %all-reduce.2 = (f32[384]{0:T(512)S(1)}, f32[384]{0:T(512)S(1)}) all-reduce(f32[384]{0:T(512)S(1)} %get-tuple-element.8, f32[384]{0:T(512)S(1)} %get-tuple-element.7), channel_id=1, replica_groups=mesh['sp'=32,'tp'=4] {'tp'}, use_global_device_ids=true, to_apply=%region_14.15 | all-reduce | flops 768 | bytes 6144 | tf_op jit(solution)/shard_map/psum | solution.py:144
  331.4 0.3 fusion.28
  331.7 3.7 %collective-permute-start = (f32[30,256]{1,0:T(8,128)S(1)}, f32[30,256]{1,0:T(8,128)S(1)}, u32[]{:S(2)}, u32[]{:S(2)}) collective-permute-start(f32[30,256]{1,0:T(8,128)S(1)} %slice.265), channel_id=1, source_target_pairs={{4,0},{8,4},{12,8},{16,12},{20,16},{24,20},{28,24},{32,28},{36,32}... | collective-permute-start | bytes 92168 | tf_op jit(solution)/shard_map/ppermute | solution.py:12
  335.4 5.2 %convolution_bitcast_fusion.1 = f32[1,2048,256]{2,1,0:T(8,128)} fusion(bf16[1152,2048]{1,0:T(8,128)(2,1)} %reshape.162, bf16[1152,256]{1,0:T(8,128)(2,1)S(1)} %copy-done.8), kind=kOutput, calls=%fused_computation.38 | convolution fusion | flops 1207959552 | bytes 7405568 | tf_op jit(solution)/shard_map/lrd,lrf->ldf/dot_general | solution.py:104
  340.6 2.7 multiply_convert_fusion.5
  343.4 0.8 multiply_convert_fusion.6
  344.2 0.8 convert_reduce_fusion
  344.9 2.7 copy.29
  (52 shorter events, 0.2 us)
Async XLA Ops:
  7.2 110.2 %copy-start = (bf16[1,2048,256]{2,1,0:T(8,128)(2,1)S(1)}, bf16[1,2048,256]{2,1,0:T(8,128)(2,1)}, u32[]{:S(2)}) copy-start(bf16[1,2048,256]{2,1,0:T(8,128)(2,1)} %param.18) | copy-start | bytes 3145732
  29.7 71.5 %all-to-all-start = ((bf16[32,36,2048]{2,1,0:T(8,128)(2,1)}), bf16[32,36,2048]{2,1,0:T(8,128)(2,1)}, u32[]{:S(2)}, u32[]{:S(2)}) async-start(bf16[32,36,2048]{2,1,0:T(8,128)(2,1)} %reshape.161), calls=%async_computation | async-start | bytes 10485760 | tf_op jit(solution)/shard_map/all_to_all | solution.py:75
  46.8 7.9 %copy-start.11 = (f32[384,2]{0,1:T(2,128)S(1)}, f32[384,2]{0,1:T(2,128)}, u32[]{:S(2)}) copy-start(f32[384,2]{0,1:T(2,128)} %param.17) | copy-start | bytes 9220
  101.2 70.7 %all-to-all-start.1 = ((bf16[32,36,2048]{2,1,0:T(8,128)(2,1)}), bf16[32,36,2048]{2,1,0:T(8,128)(2,1)}, u32[]{:S(2)}, u32[]{:S(2)}) async-start(bf16[32,36,2048]{2,1,0:T(8,128)(2,1)} %multiply_convert_fusion), calls=%async_computation.1 | async-start | bytes 10485760 | tf_op jit(solution)/shard_map/all_to_all | solution.py:76
  110.0 141.9 %reduce-scatter.2.cloned.1.call-start = ((), (), s32[]{:S(2)}) async-start(), calls=%async_computation.5 | async-start | bytes 6553600 | tf_op jit(solution)/shard_map/reduce_scatter | solution.py:117
  117.4 4.9 %copy-start.1 = (bf16[1152,2048]{1,0:T(8,128)(2,1)S(1)}, bf16[1152,2048]{1,0:T(8,128)(2,1)}, u32[]{:S(2)}) copy-start(bf16[1152,2048]{1,0:T(8,128)(2,1)} %reshape.162) | copy-start | bytes 14155780
  117.4 4.9 %copy-start.4 = (bf16[1,2048,256]{2,1,0:T(8,128)(2,1)S(1)}, bf16[1,2048,256]{2,1,0:T(8,128)(2,1)}, u32[]{:S(2)}) copy-start(bf16[1,2048,256]{2,1,0:T(8,128)(2,1)} %param.19) | copy-start | bytes 3145732
  124.8 54.3 %copy-start.12 = (bf16[1,256,2048]{2,1,0:T(8,128)(2,1)S(1)}, bf16[1,256,2048]{2,1,0:T(8,128)(2,1)}, u32[]{:S(2)}) copy-start(bf16[1,256,2048]{2,1,0:T(8,128)(2,1)} %param.20) | copy-start | bytes 3145732
  183.8 1.5 copy-start.2
  183.8 1.5 copy-start.7
  251.9 27.0 %all-to-all-start.2 = ((bf16[32,36,512]{2,1,0:T(8,128)(2,1)}), bf16[32,36,512]{2,1,0:T(8,128)(2,1)S(1)}, u32[]{:S(2)}, u32[]{:S(2)}) async-start(bf16[32,36,512]{2,1,0:T(8,128)(2,1)} %reduce-scatter.2.cloned.1.call-done), calls=%async_computation.3 | async-start | bytes 2621440 | tf_op jit(solution)/shard_map/all_to_all | solution.py:120
  259.6 50.0 %all-gather.2.cloned.1.call-start = ((), (), s32[]{:S(2)}) async-start(), calls=%async_computation.6 | async-start | bytes 1966080 | tf_op jit(solution)/shard_map/all_gather | solution.py:127
  282.8 10.9 %copy-start.10 = (f32[31,256]{1,0:T(8,128)S(1)}, f32[31,256]{1,0:T(8,128)}, u32[]{:S(2)}) copy-start(f32[31,256]{1,0:T(8,128)} %param.24) | copy-start | bytes 95236
  284.7 2.0 copy-start.6
  284.7 9.1 %copy-start.3 = (bf16[1152,256]{1,0:T(8,128)(2,1)S(1)}, bf16[1152,256]{1,0:T(8,128)(2,1)}, u32[]{:S(2)}) copy-start(bf16[1152,256]{1,0:T(8,128)(2,1)} %copy-done.2) | copy-start | bytes 1769476
  284.7 14.5 %slice-start = ((s8[4718592]{0:T(1024)(128)(4,1)}), s8[524288]{0:T(1024)(128)(4,1)S(1)}, s32[]{:S(2)}) async-start(s8[4718592]{0:T(1024)(128)(4,1)} %bitcast.87), calls=%async_computation.7 | async-start | bytes 1048576
  293.8 5.4 %slice-start.1 = ((s8[4718592]{0:T(1024)(128)(4,1)}), s8[4194304]{0:T(1024)(128)(4,1)S(1)}, s32[]{:S(2)}) async-start(s8[4718592]{0:T(1024)(128)(4,1)} %bitcast.87), calls=%async_computation.8 | async-start | bytes 8388608
  293.8 5.4 %copy-start.15 = (f32[1152,256]{1,0:T(8,128)S(1)}, f32[1152,256]{1,0:T(8,128)}, u32[]{:S(2)}) copy-start(f32[1152,256]{1,0:T(8,128)} %fusion.6) | copy-start | bytes 3538948
  293.8 5.4 %copy-start.16 = (f32[1152,256]{1,0:T(8,128)S(1)}, f32[1152,256]{1,0:T(8,128)}, u32[]{:S(2)}) copy-start(f32[1152,256]{1,0:T(8,128)} %fusion.9) | copy-start | bytes 3538948
  299.2 10.4 %copy-start.13 = (f32[256]{0:T(256)S(1)}, f32[256]{0:T(256)}, u32[]{:S(2)}) copy-start(f32[256]{0:T(256)} %param.26) | copy-start | bytes 3076
  299.3 10.4 %copy-start.14 = (f32[256]{0:T(256)S(1)}, f32[256]{0:T(256)}, u32[]{:S(2)}) copy-start(f32[256]{0:T(256)} %param.25) | copy-start | bytes 3076
  312.9 31.2 %all-to-all-start.3 = ((bf16[32,64,256]{2,1,0:T(8,128)(2,1)}), bf16[32,64,256]{2,1,0:T(8,128)(2,1)S(1)}, u32[]{:S(2)}, u32[]{:S(2)}) async-start(bf16[32,64,256]{2,1,0:T(8,128)(2,1)} %bitcast.7), calls=%async_computation.4 | async-start | bytes 2097152 | tf_op jit(solution)/shard_map/all_to_all | solution.py:23
  320.8 14.6 %copy-start.8 = (bf16[1152,256]{1,0:T(8,128)(2,1)S(1)}, bf16[1152,256]{1,0:T(8,128)(2,1)}, u32[]{:S(2)}) copy-start(bf16[1152,256]{1,0:T(8,128)(2,1)} %copy-done.7) | copy-start | bytes 1769476
  331.6 9.0 %copy-start.5 = (bf16[384,256]{1,0:T(8,128)(2,1)S(1)}, bf16[384,256]{1,0:T(8,128)(2,1)}, u32[]{:S(2)}) copy-start(bf16[384,256]{1,0:T(8,128)(2,1)} %param.23) | copy-start | bytes 589828
  331.7 9.0 %copy-start.9 = (bf16[384,256]{1,0:T(8,128)(2,1)S(1)}, bf16[384,256]{1,0:T(8,128)(2,1)}, u32[]{:S(2)}) copy-start(bf16[384,256]{1,0:T(8,128)(2,1)} %param.22) | copy-start | bytes 589828
  331.7 8.9 %collective-permute-start = (f32[30,256]{1,0:T(8,128)S(1)}, f32[30,256]{1,0:T(8,128)S(1)}, u32[]{:S(2)}, u32[]{:S(2)}) collective-permute-start(f32[30,256]{1,0:T(8,128)S(1)} %slice.265), channel_id=1, source_target_pairs={{4,0},{8,4},{12,8},{16,12},{20,16},{24,20},{28,24},{32,28},{36,32}... | collective-permute-start | bytes 92168 | tf_op jit(solution)/shard_map/ppermute | solution.py:12
Sparse Core Ops, SparseCore 0:
  196.2 55.6 reduce-scatter.1
  286.9 22.7 all-gather.1
where the time goes:
time: 356 us; the launch traced here: 354 us
  waiting for transfers between devices  164 us (46%)
  local copies, waits for them, and re-layouts  68.4 us (19%)
  starting transfers between devices  38 us (11%)
  matrix products  36.4 us (10%)
  other arithmetic  18.3 us (5%)
  blocking collectives  14.8 us (4%)
  between operations  14.5 us (4%)
    reduce_scatter x1, waiting for transfers between devices, on_device(): lax.psum_scatter(partial_low, 'tp', scatter_dimension=2, tiled=True)  55.8 us
    all_to_all x1, waiting for transfers between devices, on_device(): lax.all_to_all(send_cot, 'sp', split_axis=0, concat_axis=0, tiled=True)  47.1 us
    all_to_all x1, waiting for transfers between devices, on_device(): lax.all_to_all(send_rows, 'sp', split_axis=0, concat_axis=0, tiled=True)  34.6 us
    all_to_all x1, waiting for transfers between devices, on_device(): lax.all_to_all(row_share.astype(jnp.bfloat16), 'sp', split_axis=0, concat...  19.2 us
    another operation x2, local copies, waits for them, and re-layouts  14.4 us
    all_to_all x1, starting transfers between devices, on_device(): lax.all_to_all(send_rows, 'sp', split_axis=0, concat_axis=0, tiled=True)  9.64 us
    all_to_all x1, starting transfers between devices, on_device(): lax.all_to_all(send_cot, 'sp', split_axis=0, concat_axis=0, tiled=True)  8.76 us
    psum x1, blocking collectives, on_device(): lax.psum((jnp.sum(norm_grad, axis=1), jnp.sum(norm_grad * normed, axis=1)...  8.01 us
  transfers between devices with their start and end apart: 7, of which 5 were waited for; matrix products, arithmetic and copies ran while one was open for 17% of the time, Pallas kernels for 0%

commit v1 on v0

v1 whole, which is shorter than its diff:
```python
import jax
import jax.numpy as jnp
from jax import lax
from jax.experimental import pallas as pl
from jax.experimental.pallas import tpu as pltpu
from jax.sharding import PartitionSpec as P

MESH = pl.DeviceIdType.MESH
bf16 = jnp.bfloat16
f32 = jnp.float32
norm_eps = 1e-06

NSP = 32
NTP = 4
ROWS = 384
D = 2048
QW = 512
FG = 256
GRP = 8
GR = 288
NT = 9


def dot(a, b, ca=1, cb=0):
    return lax.dot_general(a, b, (((ca,), (cb,)), ((), ())), preferred_element_type=f32)


def iota(shape, dim):
    return lax.broadcasted_iota(jnp.int32, shape, dim)


def moe_kernel(
    x_ref,
    c_ref,
    routes_ref,
    weight_ref,
    wg_ref,
    wu_ref,
    wd_ref,
    gg_ref,
    ug_ref,
    dg_ref,
    resid_ref,
    rank_ref,
    wsel_ref,
    ohm_ref,
    ohr_ref,
    send_ref,
    got_ref,
    rows_ref,
    hid_ref,
    part_ref,
    pair_ref,
    back_ref,
    home_ref,
    flat_ref,
    flatr_ref,
    exo_ref,
    exi_ref,
    ag_ref,
    fsend,
    frecv,
    xfsend,
    xfrecv,
    xbsend,
    xbrecv,
    bsend,
    brecv,
    esend,
    erecv,
    asend,
    arecv,
):
    me = lax.axis_index("sp")
    x = lax.axis_index("tp")
    z, y, core = me // 8, (me // 2) % 4, me % 2
    right, left = (x + 1) % NTP, (x + 3) % NTP

    def peer_at(dz, m):
        return ((z + dz) % 4) * 8 + ((y + m // 2) % 4) * 2 + (core + m % 2) % 2

    def source_at(dz, m):
        return ((z + 4 - dz) % 4) * 8 + ((y + 4 - m // 2) % 4) * 2 + (core + m % 2) % 2

    def quarter(j):
        return (x + j) % NTP

    barrier = pltpu.get_barrier_semaphore()

    @pl.loop(1, NSP)
    def _(k):
        pl.semaphore_signal(
            barrier, inc=1, device_id=(peer_at(k // 8, k % 8), x), device_id_type=MESH
        )

    for side in (left, right):
        pl.semaphore_signal(barrier, inc=1, device_id=(me, side), device_id_type=MESH)

    r0, r1 = routes_ref[0:1, :], routes_ref[1:2, :]
    names = iota((NSP, ROWS), 0)
    m0, m1 = r0 == names, r1 == names
    member = jnp.where(m0 | m1, 1.0, 0.0).astype(bf16)
    before = jnp.where(iota((ROWS, ROWS), 0) < iota((ROWS, ROWS), 1), 1.0, 0.0).astype(bf16)
    rank = dot(member, before)
    rank_ref[...] = jnp.where(m0 | m1, rank, -1.0).astype(jnp.int32)
    wsel_ref[...] = jnp.where(m0, weight_ref[0:1, :], jnp.where(m1, weight_ref[1:2, :], 0.0))

    @pl.loop(0, NSP // GRP)
    def _(g):
        ranks = rank_ref[pl.ds(pl.multiple_of(g * GRP, GRP), GRP), :]
        wsel = wsel_ref[pl.ds(pl.multiple_of(g * GRP, GRP), GRP), :]
        ohs, ws, ohrs, wrs = [], [], [], []
        for i in range(GRP):
            one = ranks[i : i + 1] == iota((32, ROWS), 0)
            ohs.append(jnp.where(one, 1.0, 0.0).astype(bf16))
            ws.append(jnp.sum(jnp.where(one, wsel[i : i + 1], 0.0), axis=1, keepdims=True))
            one = ranks[i : i + 1] == 32 + iota((16, ROWS), 0) % 4
            ohrs.append(jnp.where(one, 1.0, 0.0).astype(bf16))
            wrs.append(jnp.sum(jnp.where(one, wsel[i : i + 1], 0.0), axis=1, keepdims=True))
        oh = jnp.concatenate(ohs, axis=0)
        ohr = jnp.concatenate(ohrs, axis=0)
        ohm_ref[pl.ds(pl.multiple_of(g * 256, 256), 256), :] = oh
        ohr_ref[pl.ds(pl.multiple_of(g * 128, 128), 128), :] = ohr
        w = jnp.concatenate(ws, axis=0)
        wr = jnp.concatenate(wrs, axis=0)
        col = (iota((128, 128), 0) % 16) // 4
        for t in range(2):
            for j in range(2):
                ref = c_ref if t else x_ref
                src = ref[:, pl.ds(pl.multiple_of(quarter(j) * QW, QW), QW)]
                main = dot(oh, src)
                rem = dot(ohr, src)
                if t:
                    main = main * w
                    rem = rem * wr
                main = main.astype(bf16)
                tail = jnp.zeros((128, 128), f32)
                for cg in range(4):
                    tail = jnp.where(col == cg, rem[:, cg * 128 : (cg + 1) * 128], tail)
                tail = tail.astype(bf16)
                for i in range(GRP):
                    for rt in range(2):
                        for ct in range(4):
                            send_ref[t, g * GRP + i, j, rt * 4 + ct] = main[
                                i * 32 + rt * 16 : i * 32 + rt * 16 + 16, ct * 128 : ct * 128 + 128
                            ]
                    send_ref[t, g * GRP + i, j, 8] = tail[i * 16 : i * 16 + 16]

    pl.semaphore_wait(barrier, NSP - 1 + 2)

    def forward_copy(t, k):
        peer = peer_at(k // 8, k % 8)
        return pltpu.make_async_remote_copy(
            src_ref=send_ref.at[t, peer],
            dst_ref=got_ref.at[t, me, 0:2],
            send_sem=fsend.at[t],
            recv_sem=frecv.at[t, k],
            device_id=(peer, x),
            device_id_type=MESH,
        )

    @pl.loop(0, 4)
    def _(dz):
        for t in range(2):

            @pl.loop(0, 8)
            def _(m):
                @pl.when(dz + m > 0)
                def _():
                    forward_copy(t, dz * 8 + m).start()

    for t in range(2):
        got_ref[t, me, 0:2] = send_ref[t, me]

    def to_side(src, t, origin, dz, side):
        return pltpu.make_async_remote_copy(
            src_ref=src,
            dst_ref=got_ref.at[t, origin, 2 + side],
            send_sem=xfsend.at[side],
            recv_sem=xfrecv.at[dz, side],
            device_id=(me, right if side else left),
            device_id_type=MESH,
        )

    def pass_on(dz):
        for t in range(2):

            @pl.loop(0, 8)
            def _(m):
                k = dz * 8 + m
                origin = source_at(dz, m)

                @pl.when(k > 0)
                def _():
                    pltpu.make_async_remote_copy(
                        src_ref=send_ref.at[t, origin],
                        dst_ref=got_ref.at[t, origin, 0:2],
                        send_sem=fsend.at[t],
                        recv_sem=frecv.at[t, k],
                        device_id=(origin, x),
                        device_id_type=MESH,
                    ).wait_recv()
                    to_side(got_ref.at[t, origin, 0], t, origin, dz, 1).start()
                    to_side(got_ref.at[t, origin, 1], t, origin, dz, 0).start()

                @pl.when(k == 0)
                def _():
                    to_side(send_ref.at[t, origin, 0], t, origin, dz, 1).start()
                    to_side(send_ref.at[t, origin, 1], t, origin, dz, 0).start()

    a = iota((128, 128), 0)
    perm_col = (a % 32) // 4 * 16 + (a // 32) * 4 + a % 4
    perm = jnp.where(iota((128, 128), 1) == perm_col, 1.0, 0.0).astype(bf16)

    def experts(dz):
        zs = (z + 4 - dz) % 4
        base = zs * GR
        first = zs * 8
        for side in range(2):
            whole = got_ref.at[:, pl.ds(first, 8), 2 + side]
            pltpu.make_async_remote_copy(
                src_ref=whole,
                dst_ref=whole,
                send_sem=xfsend.at[side],
                recv_sem=xfrecv.at[dz, side],
                device_id=(me, right if side else left),
                device_id_type=MESH,
            ).wait_recv()
        for t in range(2):
            for r in range(4):
                lane = quarter(r) * QW

                @pl.loop(0, 8)
                def _(i):
                    for rt in range(2):
                        for ct in range(4):
                            rows_ref[
                                t,
                                pl.ds(pl.multiple_of(base + i * 32 + rt * 16, 16), 16),
                                pl.ds(pl.multiple_of(lane + ct * 128, 128), 128),
                            ] = got_ref[t, first + i, r, rt * 4 + ct]

                rem = dot(perm, got_ref[t, pl.ds(first, 8), r, 8].reshape(128, 128)).astype(bf16)
                for cg in range(4):
                    rows_ref[
                        t,
                        pl.ds(pl.multiple_of(base + 256, 16), 32),
                        pl.ds(pl.multiple_of(lane + cg * 128, 128), 128),
                    ] = rem[cg * 32 : cg * 32 + 32]
        span = pl.ds(pl.multiple_of(base, 32), GR)
        tok = rows_ref[0, span, :]
        pre_gate = dot(tok, wg_ref[...])
        pre_up = dot(tok, wu_ref[...])
        hidden_grad = dot(rows_ref[1, span, :], wd_ref[...], 1, 1)
        sig = jax.nn.sigmoid(pre_gate)
        act = pre_gate * sig
        hid_ref[0, span, :] = (act * pre_up).astype(bf16)
        gate_pre = (hidden_grad * pre_up * sig * (1.0 + pre_gate * (1.0 - sig))).astype(bf16)
        up_pre = (hidden_grad * act).astype(bf16)
        hid_ref[1, span, :] = gate_pre
        hid_ref[2, span, :] = up_pre
        for r in (2, 3, 0, 1):
            cols = pl.ds(pl.multiple_of(quarter(r) * QW, QW), QW)
            part = dot(gate_pre, wg_ref[cols, :], 1, 1) + dot(up_pre, wu_ref[cols, :], 1, 1)
            part = part.astype(bf16)
            for i in range(8):
                for rt in range(2):
                    for ct in range(4):
                        part_ref[r, first + i, rt * 4 + ct] = part[
                            i * 32 + rt * 16 : i * 32 + rt * 16 + 16, ct * 128 : ct * 128 + 128
                        ]
            stack = jnp.concatenate(
                [part[256:GR, cg * 128 : cg * 128 + 128] for cg in range(4)], axis=0
            )
            rem = dot(perm, stack, 0, 0).astype(bf16)
            for i in range(8):
                part_ref[r, first + i, 8] = rem[i * 16 : i * 16 + 16]
            if r == 3:
                for side in range(2):
                    pair_copy(dz, side).start()

    def pair_copy(dz, side):
        group = pl.ds(((z + 4 - dz) % 4) * 8, 8)
        return pltpu.make_async_remote_copy(
            src_ref=part_ref.at[3 - side, group],
            dst_ref=pair_ref.at[side, group],
            send_sem=xbsend.at[dz, side],
            recv_sem=xbrecv.at[dz, side],
            device_id=(me, right if side else left),
            device_id_type=MESH,
        )

    def back_copy(dz, m):
        origin = source_at(dz, m)
        return pltpu.make_async_remote_copy(
            src_ref=back_ref.at[origin],
            dst_ref=home_ref.at[me],
            send_sem=bsend.at[dz],
            recv_sem=brecv.at[dz],
            device_id=(origin, x),
            device_id_type=MESH,
        )

    def send_back(dz):
        for side in range(2):
            pair_copy(dz, side).wait_recv()

        @pl.loop(0, 8)
        def _(m):
            origin = source_at(dz, m)
            for j in range(2):
                both = part_ref[j, origin].astype(f32) + pair_ref[j, origin].astype(f32)
                back_ref[origin, j] = both.astype(bf16)

        @pl.loop(0, 8)
        def _(m):
            @pl.when(dz + m > 0)
            def _():
                back_copy(dz, m).start()

            @pl.when(dz + m == 0)
            def _():
                home_ref[me] = back_ref[me]

    @pl.loop(0, 6)
    def _(step):
        @pl.when(step < 4)
        def _():
            pass_on(step)

        @pl.when((step > 0) & (step < 5))
        def _():
            experts(step - 1)

        @pl.when(step > 1)
        def _():
            send_back(step - 2)

    @pl.loop(0, 4)
    def _(g):
        cols = pl.ds(pl.multiple_of(g * QW, QW), QW)
        tok = rows_ref[0, :, cols]
        gg_ref[cols, :] = dot(tok, hid_ref[1], 0, 0)
        ug_ref[cols, :] = dot(tok, hid_ref[2], 0, 0)
        dg_ref[:, cols] = dot(hid_ref[0], rows_ref[1, :, cols], 0, 0)

    for dz in range(4):
        group = pl.ds(((z + dz) % 4) * 8, 8)
        span = home_ref.at[pl.ds(0, 7)] if dz == 0 else home_ref.at[group]
        pltpu.make_async_remote_copy(
            src_ref=span,
            dst_ref=span,
            send_sem=bsend.at[dz],
            recv_sem=brecv.at[dz],
            device_id=(peer_at(1, 0), x),
            device_id_type=MESH,
        ).wait_recv()

    @pl.loop(0, NSP)
    def _(e):
        for j in range(2):
            for rt in range(2):
                for ct in range(4):
                    flat_ref[
                        pl.ds(pl.multiple_of(e * 32 + rt * 16, 16), 16),
                        pl.ds(j * QW + ct * 128, 128),
                    ] = home_ref[e, j, rt * 4 + ct]
            flatr_ref[pl.ds(pl.multiple_of(e * 16, 16), 16), pl.ds(j * 128, 128)] = home_ref[e, j, 8]

    rem_group = (iota((512, 1), 0) % 16) // 4
    sums = []
    for j in range(2):
        main = dot(ohm_ref[...], flat_ref[:, j * QW : (j + 1) * QW], 0, 0)
        tails = []
        for cg in range(4):
            tail = jnp.where(
                rem_group == cg, flatr_ref[:, j * 128 : (j + 1) * 128].astype(f32), 0.0
            ).astype(bf16)
            tails.append(tail)
        tail = dot(ohr_ref[...], jnp.concatenate(tails, axis=1), 0, 0)
        sums.append(main + tail)
    exo_ref[0] = sums[0][:, 256:].astype(bf16)
    exo_ref[1] = sums[1][:, :256].astype(bf16)

    def exchange(side):
        return pltpu.make_async_remote_copy(
            src_ref=exo_ref.at[side],
            dst_ref=exi_ref.at[side],
            send_sem=esend.at[side],
            recv_sem=erecv.at[side],
            device_id=(me, right if side else left),
            device_id_type=MESH,
        )

    for side in range(2):
        exchange(side).start()
    for side in range(2):
        exchange(side).wait_recv()
    cot0 = c_ref[:, pl.ds(pl.multiple_of(quarter(0) * QW, 256), 256)].astype(f32)
    cot1 = c_ref[:, pl.ds(pl.multiple_of(quarter(1) * QW + 256, 256), 256)].astype(f32)
    ag_ref[0, 0] = (cot0 + (sums[0][:, :256] + exi_ref[1].astype(f32))).astype(bf16)
    ag_ref[0, 1] = (cot1 + (sums[1][:, 256:] + exi_ref[0].astype(f32))).astype(bf16)

    def gather(side):
        return pltpu.make_async_remote_copy(
            src_ref=ag_ref.at[0],
            dst_ref=ag_ref.at[3 if side else 1],
            send_sem=asend.at[side],
            recv_sem=arecv.at[side],
            device_id=(me, right if side else left),
            device_id_type=MESH,
        )

    def gather_far(side):
        return pltpu.make_async_remote_copy(
            src_ref=ag_ref.at[3 if side else 1, 1 - side],
            dst_ref=ag_ref.at[2, 1 - side],
            send_sem=asend.at[2 + side],
            recv_sem=arecv.at[2 + side],
            device_id=(me, right if side else left),
            device_id_type=MESH,
        )

    def place(o):
        resid_ref[:, pl.ds(pl.multiple_of(quarter(o) * QW, 256), 256)] = ag_ref[o, 0]
        resid_ref[:, pl.ds(pl.multiple_of(quarter(o + 1) * QW + 256, 256), 256)] = ag_ref[o, 1]

    for side in range(2):
        gather(side).start()
    place(0)
    for side in range(2):
        gather(side).wait_recv()
        gather_far(side).start()
    place(1)
    place(3)
    for side in range(2):
        gather_far(side).wait_recv()
    place(2)

    for side in range(2):
        exchange(side).wait_send()
        gather(side).wait_send()
        gather_far(side).wait_send()
        whole = got_ref.at[:, :, side]
        pltpu.make_async_remote_copy(
            src_ref=whole,
            dst_ref=whole,
            send_sem=xfsend.at[side],
            recv_sem=xfrecv.at[0, side],
            device_id=(me, right if side else left),
            device_id_type=MESH,
        ).wait_send()
        for dz in range(4):
            pair_copy(dz, side).wait_send()
    for t in range(2):
        whole = send_ref.at[t, pl.ds(0, NSP - 1)]
        pltpu.make_async_remote_copy(
            src_ref=whole,
            dst_ref=whole,
            send_sem=fsend.at[t],
            recv_sem=frecv.at[t, 0],
            device_id=(peer_at(1, 0), x),
            device_id_type=MESH,
        ).wait_send()
    for dz in range(4):
        span = back_ref.at[pl.ds(0, 7 if dz == 0 else 8)]
        pltpu.make_async_remote_copy(
            src_ref=span,
            dst_ref=span,
            send_sem=bsend.at[dz],
            recv_sem=brecv.at[dz],
            device_id=(peer_at(1, 0), x),
            device_id_type=MESH,
        ).wait_send()


def moe(expert_input, cotangent, routes, route_weight, wg, wu, wd):
    dma = pltpu.SemaphoreType.DMA
    vmem = pl.BlockSpec(memory_space=pltpu.VMEM)
    return pl.pallas_call(
        moe_kernel,
        out_shape=(
            jax.ShapeDtypeStruct((D, FG), f32),
            jax.ShapeDtypeStruct((D, FG), f32),
            jax.ShapeDtypeStruct((FG, D), f32),
            jax.ShapeDtypeStruct((ROWS, D), bf16),
        ),
        in_specs=[vmem] * 7,
        out_specs=(vmem,) * 4,
        scratch_shapes=[
            pltpu.VMEM((NSP, ROWS), jnp.int32),
            pltpu.VMEM((NSP, ROWS), f32),
            pltpu.VMEM((1024, ROWS), bf16),
            pltpu.VMEM((512, ROWS), bf16),
            pltpu.VMEM((2, NSP, 2, NT, 16, 128), bf16),
            pltpu.VMEM((2, NSP, 4, NT, 16, 128), bf16),
            pltpu.VMEM((2, 4 * GR, D), bf16),
            pltpu.VMEM((3, 4 * GR, FG), bf16),
            pltpu.VMEM((4, NSP, NT, 16, 128), bf16),
            pltpu.VMEM((2, NSP, NT, 16, 128), bf16),
            pltpu.VMEM((NSP, 2, NT, 16, 128), bf16),
            pltpu.VMEM((NSP, 2, NT, 16, 128), bf16),
            pltpu.VMEM((1024, 1024), bf16),
            pltpu.VMEM((512, 256), bf16),
            pltpu.VMEM((2, ROWS, 256), bf16),
            pltpu.VMEM((2, ROWS, 256), bf16),
            pltpu.VMEM((4, 2, ROWS, 256), bf16),
            dma((2,)),
            dma((2, NSP)),
            dma((2,)),
            dma((4, 2)),
            dma((4, 2)),
            dma((4, 2)),
            dma((4,)),
            dma((4,)),
            dma((2,)),
            dma((2,)),
            dma((4,)),
            dma((4,)),
        ],
        compiler_params=pltpu.CompilerParams(
            collective_id=0, has_side_effects=True, vmem_limit_bytes=66000000
        ),
        name="moe",
    )(expert_input, cotangent, routes.T, route_weight.T, wg, wu, wd)


def passed_along(value, axis, steps):
    count = lax.axis_size(axis)
    leading, last = (max(0, -steps), min(count, count - steps))
    return lax.ppermute(value, axis, [(source, source + steps) for source in range(leading, last)])


def cut_along(x, dim, size):
    lengths = x.shape
    tiles = x.reshape(*lengths[:dim], size, lengths[dim] // size, *lengths[dim + 1 :])
    return jnp.moveaxis(tiles, dim, 0)


def sent_and_summed(x, axis, dim):
    size = lax.axis_size(axis)
    tiles = lax.all_to_all(cut_along(x, dim, size), axis, 0, 0, tiled=True)
    return jnp.sum(tiles.astype(jnp.float32), axis=0)


def on_device(
    expert_input,
    cotangent,
    routes,
    route_weight,
    expert_gate,
    expert_up,
    expert_down,
    conv_out,
    conv_value,
    conv_gate,
    conv_taps,
    norm_gain,
    norm_bias,
    out_weight,
):
    tp_count = lax.axis_size("tp")
    tok_rows, model_width = expert_input.shape
    gate_grad, up_grad, down_grad, resid_grad = moe(
        expert_input, cotangent, routes, route_weight, expert_gate[0], expert_up[0], expert_down[0]
    )
    gate_grad, up_grad, down_grad = gate_grad[None], up_grad[None], down_grad[None]
    mix_grad = lax.dot_general(
        resid_grad, out_weight, (((1,), (1,)), ((), ())), preferred_element_type=jnp.float32
    )
    channels = conv_out.shape[1] * tp_count
    conv_vals = conv_out.astype(jnp.float32)
    row_sum, row_square = lax.psum(
        (jnp.sum(conv_vals, axis=1), jnp.sum(conv_vals * conv_vals, axis=1)), "tp"
    )
    row_mean = (row_sum / channels)[:, None]
    row_var = (row_square / channels)[:, None] - row_mean * row_mean
    row_rstd = lax.rsqrt(row_var + norm_eps)
    normed = (conv_vals - row_mean) * row_rstd
    norm_pre = normed * norm_gain[None, :] + norm_bias[None, :]
    norm_sig = jax.nn.sigmoid(norm_pre)
    conv_act = (norm_pre * norm_sig).astype(jnp.bfloat16)
    norm_grad = mix_grad * norm_sig * (1.0 + norm_pre * (1.0 - norm_sig)) * norm_gain[None, :]
    grad_sum, grad_dot = lax.psum(
        (jnp.sum(norm_grad, axis=1), jnp.sum(norm_grad * normed, axis=1)), "tp"
    )
    conv_grad = row_rstd * (
        norm_grad - (grad_sum / channels)[:, None] - normed * (grad_dot / channels)[:, None]
    )
    taps_count = conv_taps.shape[0]
    next_rows = passed_along(conv_grad[: taps_count - 1], "sp", -1)
    extended = jnp.concatenate([conv_grad, next_rows], axis=0)
    glu_grad = jnp.zeros_like(conv_grad)
    for lag_index in range(taps_count):
        begin = taps_count - 1 - lag_index
        glu_grad = glu_grad + conv_taps[lag_index][None, :] * extended[begin : begin + tok_rows]
    gate_sig_in = jax.nn.sigmoid(conv_gate.astype(jnp.float32))
    value_grad = (glu_grad * gate_sig_in).astype(jnp.bfloat16)
    gate_in_grad = (
        glu_grad * conv_value.astype(jnp.float32) * gate_sig_in * (1.0 - gate_sig_in)
    ).astype(jnp.bfloat16)
    projected = sent_and_summed(
        lax.dot_general(
            resid_grad, conv_act, (((0,), (0,)), ((), ())), preferred_element_type=jnp.float32
        ).astype(jnp.bfloat16),
        "sp",
        0,
    )
    out_weight_grad = projected.T
    return (gate_grad, up_grad, down_grad, resid_grad, out_weight_grad, value_grad, gate_in_grad)


def solution(mesh):
    return jax.shard_map(
        on_device,
        mesh=mesh,
        in_specs=(
            P("sp", None),
            P("sp", None),
            P("sp", None),
            P("sp", None),
            P("sp", None, "tp"),
            P("sp", None, "tp"),
            P("sp", "tp", None),
            P("sp", "tp"),
            P("sp", "tp"),
            P("sp", "tp"),
            P(None, "tp"),
            P("tp"),
            P("tp"),
            P("tp", None),
        ),
        out_specs=(
            P("sp", None, "tp"),
            P("sp", None, "tp"),
            P("sp", "tp", None),
            P("sp", None),
            P("tp", "sp"),
            P("sp", "tp"),
            P("sp", "tp"),
        ),
        check_vma=False,
    )
```

time: 356 us -> 216 us (0.61)
  waiting for transfers between devices: 164 us -> 10.9 us
  Pallas kernels: 0 us -> 151 us
  local copies, waits for them, and re-layouts: 68.4 us -> 8.68 us
  matrix products: 36.4 us -> 4.48 us
  starting transfers between devices: 38 us -> 15.6 us
  between operations: 14.5 us -> 0.8 us
  other arithmetic: 18.3 us -> 7.65 us
    pallas_call x0 -> x1, Pallas kernels: none -> 151 us  [moe(): pl.pallas_call(moe_kernel, out_shape=(jax.ShapeDtypeStruct((D, FG), f32),...]
    all_to_all x3 -> x0, waiting for transfers between devices: 101 us -> none  [the longest x1 47.1 us: on_device(): lax.all_to_all(send_cot, 'sp', split_axis=0, concat_axis=0, tiled=True)]
    reduce_scatter x1 -> x0, waiting for transfers between devices: 55.8 us -> none  [on_device(): lax.psum_scatter(partial_low, 'tp', scatter_dimension=2, tiled=True)]
    dot_general x8 -> x0, matrix products: 30.6 us -> none  [the longest x1 5.38 us: on_device(): jnp.einsum('lrd,lrf->ldf', slot_rows, gate_pre, preferred_element_type=jn...]
    all_to_all x3 -> x0, starting transfers between devices: 26.2 us -> none  [the longest x1 9.64 us: on_device(): lax.all_to_all(send_rows, 'sp', split_axis=0, concat_axis=0, tiled=True)]
    gather x4 -> x0, local copies, waits for them, and re-layouts: 19.2 us -> none  [the longest x1 5.98 us: on_device(): padded_cot[token_of].astype(jnp.float32) * padded_weight[slot_ids][:, None]]
    convert_element_type x3 -> x0, local copies, waits for them, and re-layouts: 16.1 us -> none  [the longest x1 7.87 us: on_device(): padded_cot[token_of].astype(jnp.float32) * padded_weight[slot_ids][:, None]]
    another operation x2 -> x0, local copies, waits for them, and re-layouts: 14.4 us -> none
  transfers between devices with their start and end apart: 7 -> 2, of which waited for: 5 -> 1; matrix products, arithmetic and copies ran while one was open for 17% -> 3% of each run, Pallas kernels for 0% -> 0%
where the time goes in v1:
time: 216 us
  Pallas kernels  151 us (70%)
  blocking collectives  17.1 us (8%)
  starting transfers between devices  15.6 us (7%)
  waiting for transfers between devices  10.9 us (5%)
  local copies, waits for them, and re-layouts  8.68 us (4%)
  other arithmetic  7.65 us (4%)
  matrix products  4.48 us (2%)
    pallas_call x1, Pallas kernels, moe(): pl.pallas_call(moe_kernel, out_shape=(jax.ShapeDtypeStruct((D, FG), f32),...  151 us
    all_to_all x1, waiting for transfers between devices, sent_and_summed(): tiles = lax.all_to_all(cut_along(x, dim, size), axis, 0, 0, tiled=True)  10.9 us
    all_to_all x1, starting transfers between devices, sent_and_summed(): tiles = lax.all_to_all(cut_along(x, dim, size), axis, 0, 0, tiled=True)  9.86 us
    psum x1, blocking collectives, on_device(): lax.psum((jnp.sum(conv_vals, axis=1), jnp.sum(conv_vals * conv_vals, axis...  9.29 us
    unnamed x26, local copies, waits for them, and re-layouts  8.64 us
    psum x1, blocking collectives, on_device(): lax.psum((jnp.sum(norm_grad, axis=1), jnp.sum(norm_grad * normed, axis=1)...  7.79 us
    ppermute x1, starting transfers between devices, passed_along(): lax.ppermute(value, axis, [(source, source + steps) for source in range(l...  5.72 us
    convert_element_type x1, other arithmetic, on_device(): gate_in_grad = (glu_grad * conv_value.astype(jnp.float32) * gate_sig_in *...  4.68 us
  transfers between devices with their start and end apart: 2, of which 1 were waited for; matrix products, arithmetic and copies ran while one was open for 3% of the time, Pallas kernels for 0%

profile of v1, /device:TPU:1, one launch (start us, length us, event | category | flops | bytes accessed | tf_op | source)
XLA Modules:
  0.0 215.8 jit_solution(10292522179107893874)
XLA Ops:
  0.6 1.1 convert_reduce_fusion.1
  1.7 9.3 %all-reduce.1 = (f32[384]{0:T(512)S(1)}, f32[384]{0:T(512)S(1)}) all-reduce(f32[384]{0:T(512)S(1)} %get-tuple-element.18, f32[384]{0:T(512)S(1)} %get-tuple-element.17), channel_id=1, replica_groups=mesh['sp'=32,'tp'=4] {'tp'}, use_global_device_ids=true, to_apply=%region_3.0 | all-reduce | flops 768 | bytes 6144 | tf_op jit(solution)/shard_map/psum | solution.py:573
  11.0 0.0 copy-start.6
  11.1 0.0 copy-start.9
  11.1 0.0 copy-start.10
  11.1 150.6 %moe.1 = (f32[2048,256]{1,0:T(8,128)}, f32[2048,256]{1,0:T(8,128)}, f32[256,2048]{1,0:T(8,128)}, bf16[384,2048]{1,0:T(8,128)(2,1)}) custom-call(bf16[384,2048]{1,0:T(8,128)(2,1)} %x_ref.1, bf16[384,2048]{1,0:T(8,128)(2,1)} %c_ref.1, s32[2,384]{1,0:T(2,128)} %bitcast.82, f32[2,384]{1,0:T(2,128)} %bitcast.83, bf16[2048,256]{1,0:T(8,128)(2,1)} %bitcast.47, ...), custom_call_target="tpu_custom_call" | custom-call | tf_op jit(solution)/shard_map/moe/pallas_call | solution.py:480
  161.7 0.0 copy-done.6
  161.7 0.0 copy-done.9
  161.7 0.0 copy-done.10
  161.7 0.0 copy-start.3
  161.7 2.6 %fusion.115 = (f32[384]{0:T(512)S(1)}, f32[384]{0:T(512)S(1)}, f32[384,256]{1,0:T(8,128)S(1)}) fusion(f32[384]{0:T(512)S(1)} %get-tuple-element.57, f32[384]{0:T(512)S(1)} %get-tuple-element.56, bf16[384,256]{1,0:T(8,128)(2,1)S(1)} %copy-done.6, f32[256]{0:T(256)S(1)} %copy-done.9, f32[256]{0:T(256)S(1)} %copy-done.10, ...), kind=kOutput, calls=%fused_computation.182 | convolution fusion | flops 404323584 | bytes 3219456 | tf_op jit(solution)/shard_map/dot_general | solution.py:568
  164.3 7.8 %all-reduce = (f32[384]{0:T(512)S(1)}, f32[384]{0:T(512)S(1)}) all-reduce(f32[384]{0:T(512)S(1)} %get-tuple-element.16, f32[384]{0:T(512)S(1)} %get-tuple-element.15), channel_id=1, replica_groups=mesh['sp'=32,'tp'=4] {'tp'}, use_global_device_ids=true, to_apply=%region_8.0 | all-reduce | flops 768 | bytes 6144 | tf_op jit(solution)/shard_map/psum | solution.py:584
  172.1 0.3 fusion.17
  172.4 5.7 %collective-permute-start = (f32[30,256]{1,0:T(8,128)S(1)}, f32[30,256]{1,0:T(8,128)S(1)}, u32[]{:S(2)}, u32[]{:S(2)}) collective-permute-start(f32[30,256]{1,0:T(8,128)S(1)} %slice.248), channel_id=1, source_target_pairs={{4,0},{8,4},{12,8},{16,12},{20,16},{24,20},{28,24},{32,28},{36,32}... | collective-permute-start | bytes 92168 | tf_op jit(solution)/shard_map/ppermute | solution.py:531
  178.1 0.0 copy-done.3
  178.2 1.9 convolution_convert_fusion
  180.0 0.0 copy-start.8
  180.0 9.9 %all-to-all-start = ((bf16[32,64,256]{2,1,0:T(8,128)(2,1)}), bf16[32,64,256]{2,1,0:T(8,128)(2,1)S(1)}, u32[]{:S(2)}, u32[]{:S(2)}) async-start(bf16[32,64,256]{2,1,0:T(8,128)(2,1)} %bitcast.8), calls=%async_computation | async-start | bytes 2097152 | tf_op jit(solution)/shard_map/all_to_all | solution.py:542
  189.9 0.0 copy-done.8
  189.9 0.0 copy-start.5
  190.0 0.0 collective-permute-done
  190.0 0.0 copy-start.7
  190.0 0.6 copy-done.7
  190.6 0.0 copy-start.2
  190.6 4.7 %multiply_convert_fusion = (bf16[384,256]{1,0:T(8,128)(2,1)}, f32[384,256]{1,0:T(8,128)S(1)}) fusion(bf16[384,256]{1,0:T(8,128)(2,1)} %param.22, bf16[384,256]{1,0:T(8,128)(2,1)} %param.23, f32[384,256]{1,0:T(8,128)S(1)} %fusion.17, f32[256]{0:T(256)S(1)} %bitcast.80, f32[30,256]{1,0:T(8,128)} %copy-done.7, f32[256]{0:T(256)S(1)} %bitcast.81, ...), kind=kLoop, calls=%fused_computation.169 | loop fusion | flops 9928704 | bytes 1438720 | tf_op jit(solution)/shard_map/convert_element_type | solution.py:601
  195.3 0.0 copy-done.5
  195.3 0.8 multiply_convert_fusion.1
  196.1 10.9 %all-to-all-done = bf16[32,64,256]{2,1,0:T(8,128)(2,1)S(1)} async-done(((bf16[32,64,256]{2,1,0:T(8,128)(2,1)}), bf16[32,64,256]{2,1,0:T(8,128)(2,1)S(1)}, u32[]{:S(2)}, u32[]{:S(2)}) %all-to-all-start) | async-done | bytes 1048608 | tf_op jit(solution)/shard_map/all_to_all | solution.py:542
  207.0 0.8 convert_reduce_fusion
  207.7 0.0 copy-done.2
  207.7 0.0 copy-start.1
  207.7 1.3 copy.25
  209.1 1.0 copy-done.1
  210.1 0.0 copy-start
  210.1 1.3 copy.26
  211.4 1.0 copy-done
  212.4 0.0 copy-start.4
  212.4 1.3 copy.27
  213.8 0.8 copy-done.4
  214.6 1.1 copy.28
  (5 shorter events, 0.1 us)
Async XLA Ops:
  11.0 150.7 %copy-start.6 = (bf16[384,256]{1,0:T(8,128)(2,1)S(1)}, bf16[384,256]{1,0:T(8,128)(2,1)}, u32[]{:S(2)}) copy-start(bf16[384,256]{1,0:T(8,128)(2,1)} %param.21) | copy-start | bytes 589828
  11.1 150.7 %copy-start.9 = (f32[256]{0:T(256)S(1)}, f32[256]{0:T(256)}, u32[]{:S(2)}) copy-start(f32[256]{0:T(256)} %param.26) | copy-start | bytes 3076
  11.1 150.7 %copy-start.10 = (f32[256]{0:T(256)S(1)}, f32[256]{0:T(256)}, u32[]{:S(2)}) copy-start(f32[256]{0:T(256)} %param.25) | copy-start | bytes 3076
  161.7 16.4 %copy-start.3 = (bf16[384,2048]{1,0:T(8,128)(2,1)S(1)}, bf16[384,2048]{1,0:T(8,128)(2,1)}, u32[]{:S(2)}) copy-start(bf16[384,2048]{1,0:T(8,128)(2,1)} %get-tuple-element.71) | copy-start | bytes 4718596
  172.4 17.6 %collective-permute-start = (f32[30,256]{1,0:T(8,128)S(1)}, f32[30,256]{1,0:T(8,128)S(1)}, u32[]{:S(2)}, u32[]{:S(2)}) collective-permute-start(f32[30,256]{1,0:T(8,128)S(1)} %slice.248), channel_id=1, source_target_pairs={{4,0},{8,4},{12,8},{16,12},{20,16},{24,20},{28,24},{32,28},{36,32}... | collective-permute-start | bytes 92168 | tf_op jit(solution)/shard_map/ppermute | solution.py:531
  180.0 9.9 %copy-start.8 = (f32[31,256]{1,0:T(8,128)S(1)}, f32[31,256]{1,0:T(8,128)}, u32[]{:S(2)}) copy-start(f32[31,256]{1,0:T(8,128)} %param.24) | copy-start | bytes 95236
  180.0 26.9 %all-to-all-start = ((bf16[32,64,256]{2,1,0:T(8,128)(2,1)}), bf16[32,64,256]{2,1,0:T(8,128)(2,1)S(1)}, u32[]{:S(2)}, u32[]{:S(2)}) async-start(bf16[32,64,256]{2,1,0:T(8,128)(2,1)} %bitcast.8), calls=%async_computation | async-start | bytes 2097152 | tf_op jit(solution)/shard_map/all_to_all | solution.py:542
  189.9 5.4 %copy-start.5 = (bf16[384,256]{1,0:T(8,128)(2,1)S(1)}, bf16[384,256]{1,0:T(8,128)(2,1)}, u32[]{:S(2)}) copy-start(bf16[384,256]{1,0:T(8,128)(2,1)} %param.23) | copy-start | bytes 589828
  190.0 0.6 copy-start.7
  190.6 17.1 %copy-start.2 = (f32[2048,256]{1,0:T(8,128)S(1)}, f32[2048,256]{1,0:T(8,128)}, u32[]{:S(2)}) copy-start(f32[2048,256]{1,0:T(8,128)} %get-tuple-element.11) | copy-start | bytes 6291460
  207.7 2.3 %copy-start.1 = (f32[2048,256]{1,0:T(8,128)S(1)}, f32[2048,256]{1,0:T(8,128)}, u32[]{:S(2)}) copy-start(f32[2048,256]{1,0:T(8,128)} %get-tuple-element.12) | copy-start | bytes 6291460
  210.1 2.3 %copy-start = (f32[256,2048]{1,0:T(8,128)S(1)}, f32[256,2048]{1,0:T(8,128)}, u32[]{:S(2)}) copy-start(f32[256,2048]{1,0:T(8,128)} %get-tuple-element.13) | copy-start | bytes 6291460
  212.4 2.2 %copy-start.4 = (bf16[384,2048]{1,0:T(8,128)(2,1)S(1)}, bf16[384,2048]{1,0:T(8,128)(2,1)}, u32[]{:S(2)}) copy-start(bf16[384,2048]{1,0:T(8,128)(2,1)} %get-tuple-element.71) | copy-start | bytes 4718596

commit v2 on v0

v2 whole, which is shorter than its diff:
```python
import jax
import jax.numpy as jnp
from jax import lax
from jax.experimental import pallas as pl
from jax.experimental.pallas import tpu as pltpu
from jax.sharding import PartitionSpec as P

MESH = pl.DeviceIdType.MESH
bf16 = jnp.bfloat16
f32 = jnp.float32
norm_eps = 1e-06

NSP = 32
NTP = 4
ROWS = 384
D = 2048
CH = 1024
KW = 31
QW = 512
FG = 256
NG = 8
GB = NSP // NG
GR = GB * 36
GM = GB * 32
GT = GB * 16
NT = 9
OW = D // NSP


def dot(a, b, ca=1, cb=0, precision=None):
    return lax.dot_general(
        a, b, (((ca,), (cb,)), ((), ())), preferred_element_type=f32, precision=precision
    )


def exact_dot(a, b, ca=1, cb=0):
    return dot(a, b, ca, cb, lax.Precision.HIGHEST)


def iota(shape, dim):
    return lax.broadcasted_iota(jnp.int32, shape, dim)


def at(start, size, step):
    return pl.ds(pl.multiple_of(start, step), size)


def layer_kernel(
    x_hbm,
    c_hbm,
    wg_hbm,
    wu_hbm,
    wd_hbm,
    ow_hbm,
    co_hbm,
    cv_hbm,
    cg_hbm,
    routes_ref,
    weight_ref,
    taps_ref,
    gain_ref,
    bias_ref,
    gg_hbm,
    ug_hbm,
    dg_hbm,
    resid_hbm,
    owg_ref,
    value_ref,
    gatein_ref,
    x_ref,
    c_ref,
    wg_ref,
    wu_ref,
    wd_ref,
    ow_ref,
    co_ref,
    cv_ref,
    cg_ref,
    gg_ref,
    ug_ref,
    dg_ref,
    resid_ref,
    rank_ref,
    wsel_ref,
    ohm_ref,
    ohr_ref,
    send_ref,
    got_ref,
    rows_ref,
    hid_ref,
    part_ref,
    pair_ref,
    back_ref,
    home_ref,
    flat_ref,
    flatr_ref,
    exo_ref,
    exi_ref,
    ag_ref,
    stat_ref,
    normed_ref,
    coef_ref,
    rstd_ref,
    act_ref,
    ext_ref,
    halo_ref,
    pso_ref,
    psi_ref,
    insem,
    outsem,
    fsend,
    frecv,
    xfsend,
    xfrecv,
    xbsend,
    xbrecv,
    bsend,
    brecv,
    esend,
    erecv,
    asend,
    arecv,
    ssend,
    srecv,
    hsend,
    hrecv,
    psend,
    precv,
):
    me = lax.axis_index("sp")
    x = lax.axis_index("tp")
    z, y, core = me // 8, (me // 2) % 4, me % 2
    right, left = (x + 1) % NTP, (x + 3) % NTP

    def offset(k):
        g, m = k // GB, k % GB
        lap, part = g * 4 // NG, g % (NG // 4)
        dz = part + (m // 2) * (NG // 4)
        return dz, (dz + lap) % 4, m % 2

    def peer_at(k):
        dz, dy, dc = offset(k)
        return ((z + dz) % 4) * 8 + ((y + dy) % 4) * 2 + (core + dc) % 2

    def source_at(k):
        dz, dy, dc = offset(k)
        return ((z + 4 - dz) % 4) * 8 + ((y + 4 - dy) % 4) * 2 + (core + dc) % 2

    def quarter(j):
        return (x + j) % NTP

    def remote(src, dst, send, recv, sp, tp):
        return pltpu.make_async_remote_copy(
            src_ref=src,
            dst_ref=dst,
            send_sem=send,
            recv_sem=recv,
            device_id=(sp, tp),
            device_id_type=MESH,
        )

    def to_left_or_right(side):
        return right if side else left

    loads = [
        pltpu.make_async_copy(src, dst, insem.at[n])
        for n, (src, dst) in enumerate(
            [
                (x_hbm, x_ref),
                (c_hbm, c_ref),
                (wg_hbm, wg_ref),
                (wu_hbm, wu_ref),
                (wd_hbm, wd_ref),
                (co_hbm, co_ref),
                (ow_hbm, ow_ref),
                (cv_hbm, cv_ref),
                (cg_hbm, cg_ref),
            ]
        )
    ]
    for load in loads:
        load.start()

    barrier = pltpu.get_barrier_semaphore()

    @pl.loop(1, NSP)
    def _(k):
        pl.semaphore_signal(barrier, inc=1, device_id=(peer_at(k), x), device_id_type=MESH)

    for j in range(1, NTP):
        pl.semaphore_signal(barrier, inc=1, device_id=(me, quarter(j)), device_id_type=MESH)

    r0, r1 = routes_ref[0:1, :], routes_ref[1:2, :]
    names = iota((NSP, ROWS), 0)
    m0, m1 = r0 == names, r1 == names
    member = jnp.where(m0 | m1, 1.0, 0.0).astype(bf16)
    before = jnp.where(iota((ROWS, ROWS), 0) < iota((ROWS, ROWS), 1), 1.0, 0.0).astype(bf16)
    rank = dot(member, before)
    rank_ref[...] = jnp.where(m0 | m1, rank, -1.0).astype(jnp.int32)
    wsel_ref[...] = jnp.where(m0, weight_ref[0:1, :], jnp.where(m1, weight_ref[1:2, :], 0.0))
    loads[0].wait()
    loads[1].wait()

    def forward_copy(t, k, peer):
        return remote(
            send_ref.at[t, k], got_ref.at[t, k, 0:2], fsend.at[t], frecv.at[t, k], peer, x
        )

    tile_col = (iota((GT, 128), 0) % 16) // 4

    @pl.loop(0, NG)
    def _(g):
        ohs, ws, ohrs, wrs = [], [], [], []
        for i in range(GB):
            peer = peer_at(g * GB + i)
            ranks = rank_ref[pl.ds(peer, 1), :]
            wsel = wsel_ref[pl.ds(peer, 1), :]
            one = ranks == iota((32, ROWS), 0)
            ohs.append(jnp.where(one, 1.0, 0.0).astype(bf16))
            ws.append(jnp.sum(jnp.where(one, wsel, 0.0), axis=1, keepdims=True))
            one = ranks == 32 + iota((16, ROWS), 0) % 4
            ohrs.append(jnp.where(one, 1.0, 0.0).astype(bf16))
            wrs.append(jnp.sum(jnp.where(one, wsel, 0.0), axis=1, keepdims=True))
        oh = jnp.concatenate(ohs, axis=0)
        ohr = jnp.concatenate(ohrs, axis=0)
        ohm_ref[at(g * GM, GM, GM), :] = oh
        ohr_ref[at(g * GT, GT, GT), :] = ohr
        w = jnp.concatenate(ws, axis=0)
        wr = jnp.concatenate(wrs, axis=0)
        for t in range(2):
            for j in range(2):
                ref = c_ref if t else x_ref
                src = ref[:, at(quarter(j) * QW, QW, QW)]
                main = dot(oh, src)
                rem = dot(ohr, src)
                if t:
                    main = main * w
                    rem = rem * wr
                main = main.astype(bf16)
                tail = jnp.zeros((GT, 128), f32)
                for cg in range(4):
                    tail = jnp.where(tile_col == cg, rem[:, cg * 128 : (cg + 1) * 128], tail)
                tail = tail.astype(bf16)
                for i in range(GB):
                    for rt in range(2):
                        for ct in range(4):
                            send_ref[t, g * GB + i, j, rt * 4 + ct] = main[
                                i * 32 + rt * 16 : i * 32 + rt * 16 + 16, ct * 128 : ct * 128 + 128
                            ]
                    send_ref[t, g * GB + i, j, 8] = tail[i * 16 : i * 16 + 16]

        @pl.when(g == 0)
        def _():
            pl.semaphore_wait(barrier, NSP - 1 + NTP - 1)

        for t in range(2):
            for i in range(GB):
                k = g * GB + i

                @pl.when(k > 0)
                def _():
                    forward_copy(t, k, peer_at(k)).start()

    for t in range(2):
        got_ref[t, 0, 0:2] = send_ref[t, 0]

    for load in loads[2:]:
        load.wait()
    ones = jnp.ones((8, FG), f32)
    spread = jnp.where(iota((8, 128), 0) == 0, 1.0, 0.0)
    spread1 = jnp.where(iota((8, 128), 0) == 1, 1.0, 0.0)

    def stat_copy(n, j):
        return remote(
            stat_ref.at[n, 0], stat_ref.at[n, NTP - j], ssend.at[n], srecv.at[n], me, quarter(j)
        )

    def stat_start(n, rows):
        stat_ref[n, 0] = rows
        for j in range(1, NTP):
            stat_copy(n, j).start()

    def stat_total(n):
        whole = stat_ref.at[n, pl.ds(1, NTP - 1)]
        remote(whole, whole, ssend.at[n], srecv.at[n], me, right).wait_recv()
        return (stat_ref[n, 0] + stat_ref[n, 1]) + (stat_ref[n, 2] + stat_ref[n, 3])

    def column(row_form, pick):
        one = exact_dot(row_form, pick, 0, 0)
        return jnp.concatenate([one, one], axis=1)

    stat_start(0, exact_dot(ones, co_ref[...].astype(f32), 1, 1))

    def to_side(src, t, k, side):
        return remote(
            src,
            got_ref.at[t, k, 2 + side],
            xfsend.at[side],
            xfrecv.at[k // GB, side],
            me,
            to_left_or_right(side),
        )

    def pass_on(g):
        for t in range(2):

            @pl.loop(0, GB)
            def _(m):
                k = g * GB + m

                @pl.when(k > 0)
                def _():
                    forward_copy(t, k, source_at(k)).wait_recv()
                    to_side(got_ref.at[t, k, 0], t, k, 1).start()
                    to_side(got_ref.at[t, k, 1], t, k, 0).start()

                @pl.when(k == 0)
                def _():
                    to_side(send_ref.at[t, k, 0], t, k, 1).start()
                    to_side(send_ref.at[t, k, 1], t, k, 0).start()

    a = iota((GT, GT), 0)
    perm_col = (a % (GB * 4)) // 4 * 16 + (a // (GB * 4)) * 4 + a % 4
    perm = jnp.where(iota((GT, GT), 1) == perm_col, 1.0, 0.0).astype(bf16)

    def experts(g):
        base = g * GR
        first = g * GB
        for side in range(2):
            whole = got_ref.at[:, pl.ds(first, GB), 2 + side]
            remote(
                whole, whole, xfsend.at[side], xfrecv.at[g, side], me, to_left_or_right(side)
            ).wait_recv()
        for t in range(2):
            for r in range(4):
                lane = quarter(r) * QW
                for i in range(GB):
                    for rt in range(2):
                        for ct in range(4):
                            rows_ref[
                                t,
                                at(base + i * 32 + rt * 16, 16, 16),
                                at(lane + ct * 128, 128, 128),
                            ] = got_ref[t, first + i, r, rt * 4 + ct]
                rem = dot(perm, got_ref[t, pl.ds(first, GB), r, 8].reshape(GT, 128)).astype(bf16)
                for cg in range(4):
                    rows_ref[
                        t, at(base + GM, GB * 4, 16), at(lane + cg * 128, 128, 128)
                    ] = rem[cg * GB * 4 : (cg + 1) * GB * 4]
        span = at(base, GR, 16)
        tok = rows_ref[0, span, :]
        pre_gate = dot(tok, wg_ref[...])
        pre_up = dot(tok, wu_ref[...])
        hidden_grad = dot(rows_ref[1, span, :], wd_ref[...], 1, 1)
        sig = jax.nn.sigmoid(pre_gate)
        act = pre_gate * sig
        hid_ref[0, span, :] = (act * pre_up).astype(bf16)
        gate_pre = (hidden_grad * pre_up * sig * (1.0 + pre_gate * (1.0 - sig))).astype(bf16)
        up_pre = (hidden_grad * act).astype(bf16)
        hid_ref[1, span, :] = gate_pre
        hid_ref[2, span, :] = up_pre
        for r in (2, 3, 0, 1):
            cols = at(quarter(r) * QW, QW, QW)
            part = dot(gate_pre, wg_ref[cols, :], 1, 1) + dot(up_pre, wu_ref[cols, :], 1, 1)
            part = part.astype(bf16)
            for i in range(GB):
                for rt in range(2):
                    for ct in range(4):
                        part_ref[r, first + i, rt * 4 + ct] = part[
                            i * 32 + rt * 16 : i * 32 + rt * 16 + 16, ct * 128 : ct * 128 + 128
                        ]
            stack = jnp.concatenate(
                [part[GM:GR, cg * 128 : cg * 128 + 128] for cg in range(4)], axis=0
            )
            rem = dot(perm, stack, 0, 0).astype(bf16)
            for i in range(GB):
                part_ref[r, first + i, 8] = rem[i * 16 : i * 16 + 16]
            if r >= 2:
                pair_copy(g, 3 - r).start()

    def pair_copy(g, side):
        group = pl.ds(g * GB, GB)
        return remote(
            part_ref.at[3 - side, group],
            pair_ref.at[side, group],
            xbsend.at[g, side],
            xbrecv.at[g, side],
            me,
            to_left_or_right(side),
        )

    def back_copy(g, m):
        k = g * GB + m
        return remote(
            back_ref.at[k], home_ref.at[k], bsend.at[g], brecv.at[g], source_at(k), x
        )

    def send_back(g):
        for side in range(2):
            pair_copy(g, side).wait_recv()

        @pl.loop(0, GB)
        def _(m):
            k = g * GB + m
            for j in range(2):
                both = part_ref[j, k].astype(f32) + pair_ref[j, k].astype(f32)
                back_ref[k, j] = both.astype(bf16)

            @pl.when(k > 0)
            def _():
                back_copy(g, m).start()

            @pl.when(k == 0)
            def _():
                home_ref[0] = back_ref[0]

    @pl.loop(0, NG + 2)
    def _(step):
        @pl.when(step < NG)
        def _():
            pass_on(step)

        @pl.when((step > 0) & (step <= NG))
        def _():
            experts(step - 1)

        @pl.when(step > 1)
        def _():
            send_back(step - 2)

    @pl.loop(0, 4)
    def _(g):
        cols = at(g * QW, QW, QW)
        tok = rows_ref[0, :, cols]
        gg_ref[cols, :] = dot(tok, hid_ref[1], 0, 0).astype(bf16)
        ug_ref[cols, :] = dot(tok, hid_ref[2], 0, 0).astype(bf16)
        dg_ref[:, cols] = dot(hid_ref[0], rows_ref[1, :, cols], 0, 0).astype(bf16)

    stores = [
        pltpu.make_async_copy(src, dst, outsem.at[n])
        for n, (src, dst) in enumerate(
            [(gg_ref, gg_hbm), (ug_ref, ug_hbm), (dg_ref, dg_hbm), (resid_ref, resid_hbm)]
        )
    ]
    for store in stores[:3]:
        store.start()

    conv = co_ref[...].astype(f32)
    mean = column(stat_total(0), spread) / CH
    centred = conv - mean
    stat_start(1, exact_dot(ones, centred * centred, 1, 1))
    var = column(stat_total(1), spread) / CH
    rstd = lax.rsqrt(var + norm_eps)
    normed = centred * rstd
    norm_pre = normed * gain_ref[...] + bias_ref[...]
    norm_sig = jax.nn.sigmoid(norm_pre)
    act_ref[...] = (norm_pre * norm_sig).astype(bf16)
    normed_ref[...] = normed
    rstd_ref[...] = rstd
    coef_ref[...] = norm_sig * (1.0 + norm_pre * (1.0 - norm_sig)) * gain_ref[...]

    for g in range(NG):
        span = home_ref.at[pl.ds(1, GB - 1)] if g == 0 else home_ref.at[pl.ds(g * GB, GB)]
        remote(span, span, bsend.at[g], brecv.at[g], peer_at(1), x).wait_recv()

    @pl.loop(0, NSP)
    def _(e):
        for j in range(2):
            for rt in range(2):
                for ct in range(4):
                    flat_ref[at(e * 32 + rt * 16, 16, 16), pl.ds(j * QW + ct * 128, 128)] = (
                        home_ref[e, j, rt * 4 + ct]
                    )
            flatr_ref[at(e * 16, 16, 16), pl.ds(j * 128, 128)] = home_ref[e, j, 8]

    rem_group = (iota((512, 1), 0) % 16) // 4
    sums = []
    for j in range(2):
        main = dot(ohm_ref[...], flat_ref[:, j * QW : (j + 1) * QW], 0, 0)
        rems = flatr_ref[:, j * 128 : (j + 1) * 128].astype(f32)
        tails = [jnp.where(rem_group == cg, rems, 0.0).astype(bf16) for cg in range(4)]
        sums.append(main + dot(ohr_ref[...], jnp.concatenate(tails, axis=1), 0, 0))
    exo_ref[0] = sums[0][:, 256:].astype(bf16)
    exo_ref[1] = sums[1][:, :256].astype(bf16)

    def exchange(side):
        return remote(
            exo_ref.at[side],
            exi_ref.at[side],
            esend.at[side],
            erecv.at[side],
            me,
            to_left_or_right(side),
        )

    for side in range(2):
        exchange(side).start()
    for side in range(2):
        exchange(side).wait_recv()
    cot0 = c_ref[:, at(quarter(0) * QW, 256, 256)].astype(f32)
    cot1 = c_ref[:, at(quarter(1) * QW + 256, 256, 256)].astype(f32)
    ag_ref[0, 0] = (cot0 + (sums[0][:, :256] + exi_ref[1].astype(f32))).astype(bf16)
    ag_ref[0, 1] = (cot1 + (sums[1][:, 256:] + exi_ref[0].astype(f32))).astype(bf16)

    def gather(side):
        return remote(
            ag_ref.at[0],
            ag_ref.at[3 if side else 1],
            asend.at[side],
            arecv.at[side],
            me,
            to_left_or_right(side),
        )

    def gather_far(side):
        return remote(
            ag_ref.at[3 if side else 1, 1 - side],
            ag_ref.at[2, 1 - side],
            asend.at[2 + side],
            arecv.at[2 + side],
            me,
            to_left_or_right(side),
        )

    def place(o):
        resid_ref[:, at(quarter(o) * QW, 256, 256)] = ag_ref[o, 0]
        resid_ref[:, at(quarter(o + 1) * QW + 256, 256, 256)] = ag_ref[o, 1]

    for side in range(2):
        gather(side).start()
    place(0)
    for side in range(2):
        gather(side).wait_recv()
        gather_far(side).start()
    place(1)
    place(3)
    for side in range(2):
        gather_far(side).wait_recv()
    place(2)
    stores[3].start()

    mix_grad = dot(resid_ref[...], ow_ref[...], 1, 1)
    norm_grad = mix_grad * coef_ref[...]
    sum_rows = exact_dot(ones, norm_grad, 1, 1)
    dot_rows = exact_dot(ones, norm_grad * normed_ref[...], 1, 1)
    stat_start(2, jnp.where(iota((8, ROWS), 0) == 0, sum_rows, dot_rows))

    def owg_copy(k, peer):
        return remote(pso_ref.at[k], psi_ref.at[k], psend.at[0], precv.at[0], peer, x)

    @pl.loop(0, 4)
    def _(g):
        cols = at(g * QW, QW, QW)
        term = dot(resid_ref[:, cols], act_ref[...], 0, 0).astype(bf16)
        for i in range(8):
            for rt in range(4):
                for ct in range(2):
                    flat_ref[
                        at((g % 2) * 512 + i * OW + rt * 16, 16, 16),
                        at((g // 2) * 256 + ct * 128, 128, 128),
                    ] = term[i * OW + rt * 16 : i * OW + rt * 16 + 16, ct * 128 : ct * 128 + 128]

    @pl.loop(0, NSP)
    def _(k):
        peer = peer_at(k)
        for rt in range(4):
            for ct in range(2):
                pso_ref[k, rt * 2 + ct] = flat_ref[
                    at((peer % 16) * OW + rt * 16, 16, 16),
                    at((peer // 16) * 256 + ct * 128, 128, 128),
                ]

        @pl.when(k > 0)
        def _():
            owg_copy(k, peer).start()

    totals = stat_total(2)
    conv_grad = rstd_ref[...] * (
        norm_grad
        - column(totals, spread) / CH
        - normed_ref[...] * (column(totals, spread1) / CH)
    )
    ext_ref[0:ROWS, :] = conv_grad

    def halo_copy(sp):
        return remote(ext_ref.at[0:32], halo_ref, hsend.at[0], hrecv.at[0], sp, x)

    @pl.when(me > 0)
    def _():
        halo_copy(me - 1).start()

    def convolve(start, rows):
        glu = jnp.zeros((rows, FG), f32)
        for lag in range(KW):
            begin = start + KW - 1 - lag
            glu = glu + taps_ref[lag : lag + 1, :] * ext_ref[begin : begin + rows, :]
        span = pl.ds(start, rows)
        gate_sig = jax.nn.sigmoid(cg_ref[span, :].astype(f32))
        value_ref[span, :] = (glu * gate_sig).astype(bf16)
        gatein_ref[span, :] = (
            glu * cv_ref[span, :].astype(f32) * gate_sig * (1.0 - gate_sig)
        ).astype(bf16)

    for start in range(0, ROWS - 32, 32):
        convolve(start, 32)

    @pl.when(me < NSP - 1)
    def _():
        halo_copy(me + 1).wait_recv()
        ext_ref[ROWS : ROWS + 32, :] = halo_ref[...]

    @pl.when(me == NSP - 1)
    def _():
        ext_ref[ROWS : ROWS + 32, :] = jnp.zeros((32, FG), f32)

    convolve(ROWS - 32, 32)

    whole = psi_ref.at[pl.ds(1, NSP - 1)]
    remote(whole, whole, psend.at[0], precv.at[0], me, right).wait_recv()
    for rt in range(4):
        for ct in range(2):
            total = pso_ref[0, rt * 2 + ct].astype(f32)
            for k in range(1, NSP):
                total = total + psi_ref[k, rt * 2 + ct].astype(f32)
            owg_ref[rt * 16 : rt * 16 + 16, ct * 128 : ct * 128 + 128] = total

    @pl.when(me > 0)
    def _():
        halo_copy(me - 1).wait_send()

    remote(whole, whole, psend.at[0], precv.at[0], me, right).wait_send()
    for n in range(3):
        sent = stat_ref.at[n, pl.ds(1, NTP - 1)]
        remote(sent, sent, ssend.at[n], srecv.at[n], me, right).wait_send()
    for side in range(2):
        exchange(side).wait_send()
        gather(side).wait_send()
        gather_far(side).wait_send()
        sent = got_ref.at[:, :, side]
        remote(sent, sent, xfsend.at[side], xfrecv.at[0, side], me, right).wait_send()
        for g in range(NG):
            pair_copy(g, side).wait_send()
    for t in range(2):
        sent = send_ref.at[t, pl.ds(0, NSP - 1)]
        remote(sent, sent, fsend.at[t], frecv.at[t, 0], me, right).wait_send()
    for g in range(NG):
        sent = back_ref.at[pl.ds(0, GB - 1 if g == 0 else GB)]
        remote(sent, sent, bsend.at[g], brecv.at[g], me, right).wait_send()
    for store in stores:
        store.wait()


def on_device(
    expert_input,
    cotangent,
    routes,
    route_weight,
    expert_gate,
    expert_up,
    expert_down,
    conv_out,
    conv_value,
    conv_gate,
    conv_taps,
    norm_gain,
    norm_bias,
    out_weight,
):
    dma = pltpu.SemaphoreType.DMA
    vmem = pl.BlockSpec(memory_space=pltpu.VMEM)
    anywhere = pl.BlockSpec(memory_space=pl.ANY)
    shape = jax.ShapeDtypeStruct
    gate_grad, up_grad, down_grad, resid_grad, projected, value_grad, gate_in_grad = pl.pallas_call(
        layer_kernel,
        out_shape=(
            shape((D, FG), bf16),
            shape((D, FG), bf16),
            shape((FG, D), bf16),
            shape((ROWS, D), bf16),
            shape((OW, FG), f32),
            shape((ROWS, FG), bf16),
            shape((ROWS, FG), bf16),
        ),
        in_specs=[anywhere] * 9 + [vmem] * 5,
        out_specs=(anywhere,) * 4 + (vmem,) * 3,
        scratch_shapes=[
            pltpu.VMEM((ROWS, D), bf16),
            pltpu.VMEM((ROWS, D), bf16),
            pltpu.VMEM((D, FG), bf16),
            pltpu.VMEM((D, FG), bf16),
            pltpu.VMEM((FG, D), bf16),
            pltpu.VMEM((FG, D), bf16),
            pltpu.VMEM((ROWS, FG), bf16),
            pltpu.VMEM((ROWS, FG), bf16),
            pltpu.VMEM((ROWS, FG), bf16),
            pltpu.VMEM((D, FG), bf16),
            pltpu.VMEM((D, FG), bf16),
            pltpu.VMEM((FG, D), bf16),
            pltpu.VMEM((ROWS, D), bf16),
            pltpu.VMEM((NSP, ROWS), jnp.int32),
            pltpu.VMEM((NSP, ROWS), f32),
            pltpu.VMEM((1024, ROWS), bf16),
            pltpu.VMEM((512, ROWS), bf16),
            pltpu.VMEM((2, NSP, 2, NT, 16, 128), bf16),
            pltpu.VMEM((2, NSP, 4, NT, 16, 128), bf16),
            pltpu.VMEM((2, NSP * 36, D), bf16),
            pltpu.VMEM((3, NSP * 36, FG), bf16),
            pltpu.VMEM((4, NSP, NT, 16, 128), bf16),
            pltpu.VMEM((2, NSP, NT, 16, 128), bf16),
            pltpu.VMEM((NSP, 2, NT, 16, 128), bf16),
            pltpu.VMEM((NSP, 2, NT, 16, 128), bf16),
            pltpu.VMEM((1024, 1024), bf16),
            pltpu.VMEM((512, 256), bf16),
            pltpu.VMEM((2, ROWS, 256), bf16),
            pltpu.VMEM((2, ROWS, 256), bf16),
            pltpu.VMEM((4, 2, ROWS, 256), bf16),
            pltpu.VMEM((3, NTP, 8, ROWS), f32),
            pltpu.VMEM((ROWS, FG), f32),
            pltpu.VMEM((ROWS, FG), f32),
            pltpu.VMEM((ROWS, FG), f32),
            pltpu.VMEM((ROWS, FG), bf16),
            pltpu.VMEM((ROWS + 32, FG), f32),
            pltpu.VMEM((32, FG), f32),
            pltpu.VMEM((NSP, 8, 16, 128), bf16),
            pltpu.VMEM((NSP, 8, 16, 128), bf16),
            dma((9,)),
            dma((4,)),
            dma((2,)),
            dma((2, NSP)),
            dma((2,)),
            dma((NG, 2)),
            dma((NG, 2)),
            dma((NG, 2)),
            dma((NG,)),
            dma((NG,)),
            dma((2,)),
            dma((2,)),
            dma((4,)),
            dma((4,)),
            dma((3,)),
            dma((3,)),
            dma((1,)),
            dma((1,)),
            dma((1,)),
            dma((1,)),
        ],
        compiler_params=pltpu.CompilerParams(
            collective_id=0, has_side_effects=True, vmem_limit_bytes=67000000
        ),
        name="layer",
    )(
        expert_input,
        cotangent,
        expert_gate[0],
        expert_up[0],
        expert_down[0],
        out_weight,
        conv_out,
        conv_value,
        conv_gate,
        routes.T,
        route_weight.T,
        conv_taps,
        norm_gain[None, :],
        norm_bias[None, :],
    )
    return (
        gate_grad[None].astype(f32),
        up_grad[None].astype(f32),
        down_grad[None].astype(f32),
        resid_grad,
        projected.T,
        value_grad,
        gate_in_grad,
    )


def solution(mesh):
    return jax.shard_map(
        on_device,
        mesh=mesh,
        in_specs=(
            P("sp", None),
            P("sp", None),
            P("sp", None),
            P("sp", None),
            P("sp", None, "tp"),
            P("sp", None, "tp"),
            P("sp", "tp", None),
            P("sp", "tp"),
            P("sp", "tp"),
            P("sp", "tp"),
            P(None, "tp"),
            P("tp"),
            P("tp"),
            P("tp", None),
        ),
        out_specs=(
            P("sp", None, "tp"),
            P("sp", None, "tp"),
            P("sp", "tp", None),
            P("sp", None),
            P("tp", "sp"),
            P("sp", "tp"),
            P("sp", "tp"),
        ),
        check_vma=False,
    )
```

time: 356 us -> 161 us (0.45)
  waiting for transfers between devices: 164 us -> 0 us
  Pallas kernels: 0 us -> 150 us
  local copies, waits for them, and re-layouts: 68.4 us -> 3.5 us
  starting transfers between devices: 38 us -> 0 us
  matrix products: 36.4 us -> 0 us
  blocking collectives: 14.8 us -> 0 us
  between operations: 14.5 us -> 0.66 us
  other arithmetic: 18.3 us -> 5.53 us
    pallas_call x0 -> x1, Pallas kernels: none -> 150 us  [on_device(): pl.pallas_call(layer_kernel, out_shape=(shape((D, FG), bf16), shape((D, F...]
    all_to_all x4 -> x0, waiting for transfers between devices: 101 us -> none  [the longest x1 47.1 us: on_device(): lax.all_to_all(send_cot, 'sp', split_axis=0, concat_axis=0, tiled=True)]
    reduce_scatter x1 -> x0, waiting for transfers between devices: 55.8 us -> none  [on_device(): lax.psum_scatter(partial_low, 'tp', scatter_dimension=2, tiled=True)]
    dot_general x10 -> x0, matrix products: 36.4 us -> none  [the longest x1 5.38 us: on_device(): jnp.einsum('lrd,lrf->ldf', slot_rows, gate_pre, preferred_element_type=jn...]
    all_to_all x4 -> x0, starting transfers between devices: 34 us -> none  [the longest x1 9.64 us: on_device(): lax.all_to_all(send_rows, 'sp', split_axis=0, concat_axis=0, tiled=True)]
    gather x4 -> x0, local copies, waits for them, and re-layouts: 19.2 us -> none  [the longest x1 5.98 us: on_device(): padded_cot[token_of].astype(jnp.float32) * padded_weight[slot_ids][:, None]]
    convert_element_type x3 -> x0, local copies, waits for them, and re-layouts: 16.1 us -> none  [the longest x1 7.87 us: on_device(): padded_cot[token_of].astype(jnp.float32) * padded_weight[slot_ids][:, None]]
    psum x2 -> x0, blocking collectives: 14.8 us -> none  [the longest x1 8.01 us: on_device(): lax.psum((jnp.sum(norm_grad, axis=1), jnp.sum(norm_grad * normed, axis=1)...]
  transfers between devices with their start and end apart: 7 -> 0, of which waited for: 5 -> 0; matrix products, arithmetic and copies ran while one was open for 17% -> 0% of each run, Pallas kernels for 0% -> 0%
where the time goes in v2:
time: 161 us; the launch traced here: 160 us
  Pallas kernels  150 us (93%)
  other arithmetic  5.53 us (3%)
  local copies, waits for them, and re-layouts  3.5 us (2%)
    pallas_call x1, Pallas kernels, on_device(): pl.pallas_call(layer_kernel, out_shape=(shape((D, FG), bf16), shape((D, F...  150 us
    convert_element_type x1, other arithmetic, on_device(): up_grad[None].astype(f32)  3.97 us
    unnamed x14, local copies, waits for them, and re-layouts  3.5 us

profile of v2, /device:TPU:1, one launch (start us, length us, event | category | flops | bytes accessed | tf_op | source)
XLA Modules:
  0.0 159.7 jit_solution(6921023182284237050)
XLA Ops:
  0.6 150.0 %layer.1 = (bf16[2048,256]{1,0:T(8,128)(2,1)}, bf16[2048,256]{1,0:T(8,128)(2,1)}, bf16[256,2048]{1,0:T(8,128)(2,1)}, bf16[384,2048]{1,0:T(8,128)(2,1)}, f32[64,2...) custom-call(bf16[384,2048]{1,0:T(8,128)(2,1)} %x_hbm.1, bf16[384,2048]{1,0:T(8,128)(2,1)} %c_hbm.1, ...), custom_call_target="tpu_custom_call" | custom-call | tf_op jit(solution)/shard_map/layer/pallas_call | solution.py:673
  150.6 0.0 copy-start.1
  150.6 4.0 %bitcast_convert_fusion.1 = (f32[1,2048,256]{2,1,0:T(8,128)}, f32[1,2048,256]{2,1,0:T(8,128)}) fusion(bf16[2048,256]{1,0:T(8,128)(2,1)} %get-tuple-element.15, bf16[2048,256]{1,0:T(8,128)(2,1)} %get-tuple-element.14), kind=kLoop, calls=%fused_computation.1 | loop fusion | flops 1048576 | bytes 6291456 | tf_op jit(solution)/shard_map/convert_element_type | solution.py:769
  154.6 0.0 copy-start
  154.6 0.0 copy-done.1
  154.6 1.6 bitcast_convert_fusion
  156.2 0.0 copy-start.4
  156.2 0.0 copy-start.3
  156.2 0.0 copy-start.2
  156.2 0.4 copy-done
  156.5 1.1 copy.25
  157.7 0.0 copy-done.4
  157.7 0.6 copy.26
  158.3 0.0 copy-done.3
  158.3 0.7 copy.27
  159.0 0.0 copy-done.2
  159.0 0.7 copy.28
Async XLA Ops:
  150.6 4.0 %copy-start.1 = (bf16[256,2048]{1,0:T(8,128)(2,1)S(1)}, bf16[256,2048]{1,0:T(8,128)(2,1)}, u32[]{:S(2)}) copy-start(bf16[256,2048]{1,0:T(8,128)(2,1)} %get-tuple-element.16) | copy-start | bytes 3145732
  154.6 1.9 %copy-start = (bf16[384,2048]{1,0:T(8,128)(2,1)S(1)}, bf16[384,2048]{1,0:T(8,128)(2,1)}, u32[]{:S(2)}) copy-start(bf16[384,2048]{1,0:T(8,128)(2,1)} %get-tuple-element.33) | copy-start | bytes 4718596
  156.2 1.5 copy-start.4
  156.2 2.1 %copy-start.3 = (bf16[384,256]{1,0:T(8,128)(2,1)S(1)}, bf16[384,256]{1,0:T(8,128)(2,1)}, u32[]{:S(2)}) copy-start(bf16[384,256]{1,0:T(8,128)(2,1)} %get-tuple-element.35) | copy-start | bytes 589828
  156.2 2.8 %copy-start.2 = (bf16[384,256]{1,0:T(8,128)(2,1)S(1)}, bf16[384,256]{1,0:T(8,128)(2,1)}, u32[]{:S(2)}) copy-start(bf16[384,256]{1,0:T(8,128)(2,1)} %get-tuple-element.36) | copy-start | bytes 589828

commit v3 on v2

--- a/solution.py
+++ b/solution.py
@@ -23,7 +23,9 @@
 GR = GB * 36
 GM = GB * 32
 GT = GB * 16
+GO = GM + GT
 NT = 9
+WHOLE = 2
 OW = D // NSP
 
 
@@ -82,9 +84,9 @@
     resid_ref,
     rank_ref,
     wsel_ref,
-    ohm_ref,
-    ohr_ref,
+    oh_ref,
     send_ref,
+    more_ref,
     got_ref,
     rows_ref,
     hid_ref,
@@ -92,8 +94,7 @@
     pair_ref,
     back_ref,
     home_ref,
-    flat_ref,
-    flatr_ref,
+    sum_ref,
     exo_ref,
     exi_ref,
     ag_ref,
@@ -110,6 +111,8 @@
     outsem,
     fsend,
     frecv,
+    msend,
+    mrecv,
     xfsend,
     xfrecv,
     xbsend,
@@ -206,10 +209,14 @@
             send_ref.at[t, k], got_ref.at[t, k, 0:2], fsend.at[t], frecv.at[t, k], peer, x
         )
 
+    def more_copy(t, slot, k, peer):
+        return remote(
+            more_ref.at[t, slot], got_ref.at[t, k, 2:4], msend.at[0], mrecv.at[t, slot], peer, x
+        )
+
     tile_col = (iota((GT, 128), 0) % 16) // 4
 
-    @pl.loop(0, NG)
-    def _(g):
+    def prepare(g):
         ohs, ws, ohrs, wrs = [], [], [], []
         for i in range(GB):
             peer = peer_at(g * GB + i)
@@ -221,37 +228,59 @@
             one = ranks == 32 + iota((16, ROWS), 0) % 4
             ohrs.append(jnp.where(one, 1.0, 0.0).astype(bf16))
             wrs.append(jnp.sum(jnp.where(one, wsel, 0.0), axis=1, keepdims=True))
-        oh = jnp.concatenate(ohs, axis=0)
-        ohr = jnp.concatenate(ohrs, axis=0)
-        ohm_ref[at(g * GM, GM, GM), :] = oh
-        ohr_ref[at(g * GT, GT, GT), :] = ohr
-        w = jnp.concatenate(ws, axis=0)
-        wr = jnp.concatenate(wrs, axis=0)
+        oh = jnp.concatenate(ohs + ohrs, axis=0)
+        oh_ref[at(g * GO, GO, 16), :] = oh
+        w = jnp.concatenate(ws + wrs, axis=0)
+        def cut_tiles(t, j, store, members):
+            ref = c_ref if t else x_ref
+            main = dot(oh, ref[:, at(quarter(j) * QW, QW, QW)])
+            if t:
+                main = main * w
+            rem = main[GM:]
+            tail = jnp.zeros((GT, 128), f32)
+            for cg in range(4):
+                tail = jnp.where(tile_col == cg, rem[:, cg * 128 : (cg + 1) * 128], tail)
+            main = main.astype(bf16)
+            tail = tail.astype(bf16)
+            for i in range(members):
+                for rt in range(2):
+                    for ct in range(4):
+                        store(
+                            i,
+                            rt * 4 + ct,
+                            main[
+                                i * 32 + rt * 16 : i * 32 + rt * 16 + 16, ct * 128 : ct * 128 + 128
+                            ],
+                        )
+                store(i, 8, tail[i * 16 : i * 16 + 16])
+
+        def more(slot, members):
+            for t in range(2):
+                for j in range(2):
+
+                    def store(i, tile, value):
+                        more_ref[t, slot + i, j, tile] = value
+
+                    cut_tiles(t, 2 + j, store, members)
+
         for t in range(2):
             for j in range(2):
-                ref = c_ref if t else x_ref
-                src = ref[:, at(quarter(j) * QW, QW, QW)]
-                main = dot(oh, src)
-                rem = dot(ohr, src)
-                if t:
-                    main = main * w
-                    rem = rem * wr
-                main = main.astype(bf16)
-                tail = jnp.zeros((GT, 128), f32)
-                for cg in range(4):
-                    tail = jnp.where(tile_col == cg, rem[:, cg * 128 : (cg + 1) * 128], tail)
-                tail = tail.astype(bf16)
-                for i in range(GB):
-                    for rt in range(2):
-                        for ct in range(4):
-                            send_ref[t, g * GB + i, j, rt * 4 + ct] = main[
-                                i * 32 + rt * 16 : i * 32 + rt * 16 + 16, ct * 128 : ct * 128 + 128
-                            ]
-                    send_ref[t, g * GB + i, j, 8] = tail[i * 16 : i * 16 + 16]
+
+                def store(i, tile, value):
+                    send_ref[t, g * GB + i, j, tile] = value
+
+                cut_tiles(t, j, store, GB)
 
         @pl.when(g == 0)
         def _():
+            more(0, 2)
+
+        @pl.when(g == 0)
+        def _():
             pl.semaphore_wait(barrier, NSP - 1 + NTP - 1)
+            for t in range(2):
+                got_ref[t, 0, 0:2] = send_ref[t, 0]
+                got_ref[t, 0, 2:4] = more_ref[t, 0]
 
         for t in range(2):
             for i in range(GB):
@@ -261,11 +290,12 @@
                 def _():
                     forward_copy(t, k, peer_at(k)).start()
 
-    for t in range(2):
-        got_ref[t, 0, 0:2] = send_ref[t, 0]
-
-    for load in loads[2:]:
-        load.wait()
+                if i == 1:
+
+                    @pl.when(g == 0)
+                    def _():
+                        more_copy(t, 1, k, peer_at(k)).start()
+
     ones = jnp.ones((8, FG), f32)
     spread = jnp.where(iota((8, 128), 0) == 0, 1.0, 0.0)
     spread1 = jnp.where(iota((8, 128), 0) == 1, 1.0, 0.0)
@@ -289,7 +319,6 @@
         one = exact_dot(row_form, pick, 0, 0)
         return jnp.concatenate([one, one], axis=1)
 
-    stat_start(0, exact_dot(ones, co_ref[...].astype(f32), 1, 1))
 
     def to_side(src, t, k, side):
         return remote(
@@ -311,13 +340,11 @@
                 @pl.when(k > 0)
                 def _():
                     forward_copy(t, k, source_at(k)).wait_recv()
+
+                @pl.when(k > 1)
+                def _():
                     to_side(got_ref.at[t, k, 0], t, k, 1).start()
                     to_side(got_ref.at[t, k, 1], t, k, 0).start()
-
-                @pl.when(k == 0)
-                def _():
-                    to_side(send_ref.at[t, k, 0], t, k, 1).start()
-                    to_side(send_ref.at[t, k, 1], t, k, 0).start()
 
     a = iota((GT, GT), 0)
     perm_col = (a % (GB * 4)) // 4 * 16 + (a // (GB * 4)) * 4 + a % 4
@@ -326,11 +353,26 @@
     def experts(g):
         base = g * GR
         first = g * GB
-        for side in range(2):
-            whole = got_ref.at[:, pl.ds(first, GB), 2 + side]
-            remote(
-                whole, whole, xfsend.at[side], xfrecv.at[g, side], me, to_left_or_right(side)
-            ).wait_recv()
+        def side_wait(start, size):
+            for side in range(2):
+                whole = got_ref.at[:, pl.ds(start, size), 2 + side]
+                remote(
+                    whole, whole, xfsend.at[side], xfrecv.at[g, side], me, to_left_or_right(side)
+                ).wait_recv()
+
+        @pl.when(g == 0)
+        def _():
+            side_wait(first + 2, GB - 2)
+
+        @pl.when(g > 0)
+        def _():
+            side_wait(first, GB)
+
+        @pl.when(g == 0)
+        def _():
+            for t in range(2):
+                more_copy(t, 1, 1, source_at(1)).wait_recv()
+
         for t in range(2):
             for r in range(4):
                 lane = quarter(r) * QW
@@ -414,13 +456,52 @@
             def _():
                 home_ref[0] = back_ref[0]
 
+    def home_wait(g):
+        @pl.when(g == 0)
+        def _():
+            span = home_ref.at[pl.ds(1, GB - 1)]
+            remote(span, span, bsend.at[g], brecv.at[g], peer_at(1), x).wait_recv()
+
+        @pl.when(g > 0)
+        def _():
+            span = home_ref.at[pl.ds(g * GB, GB)]
+            remote(span, span, bsend.at[g], brecv.at[g], peer_at(1), x).wait_recv()
+
+    def combine(g, js=(0, 1)):
+        oh = oh_ref[at(g * GO, GO, 16), :]
+        for j in js:
+            rows = []
+            for i in range(GB):
+                for rt in range(2):
+                    rows.append(
+                        jnp.concatenate(
+                            [home_ref[g * GB + i, j, rt * 4 + ct] for ct in range(4)], axis=1
+                        )
+                    )
+            rem = home_ref[pl.ds(g * GB, GB), j, 8].reshape(GT, 128).astype(f32)
+            tails = [jnp.where(tile_col == cg, rem, 0.0).astype(bf16) for cg in range(4)]
+            rows.append(jnp.concatenate(tails, axis=1))
+            sum_ref[:, j * QW : (j + 1) * QW] += dot(oh, jnp.concatenate(rows, axis=0), 0, 0)
+
+    sum_ref[...] = jnp.zeros_like(sum_ref)
+
+    @pl.loop(0, NG)
+    def _(g):
+        prepare(g)
+
     @pl.loop(0, NG + 2)
     def _(step):
         @pl.when(step < NG)
         def _():
             pass_on(step)
 
-        @pl.when((step > 0) & (step <= NG))
+        @pl.when(step == 0)
+        def _():
+            for load in loads[2:]:
+                load.wait()
+            stat_start(0, exact_dot(ones, co_ref[...].astype(f32), 1, 1))
+
+        @pl.when((step > 0) & (step < NG + 1))
         def _():
             experts(step - 1)
 
@@ -428,9 +509,8 @@
         def _():
             send_back(step - 2)
 
-    @pl.loop(0, 4)
-    def _(g):
-        cols = at(g * QW, QW, QW)
+    def weight_grads(g):
+        cols = pl.ds(g * QW, QW)
         tok = rows_ref[0, :, cols]
         gg_ref[cols, :] = dot(tok, hid_ref[1], 0, 0).astype(bf16)
         ug_ref[cols, :] = dot(tok, hid_ref[2], 0, 0).astype(bf16)
@@ -442,8 +522,7 @@
             [(gg_ref, gg_hbm), (ug_ref, ug_hbm), (dg_ref, dg_hbm), (resid_ref, resid_hbm)]
         )
     ]
-    for store in stores[:3]:
-        store.start()
+    weight_grads(0)
 
     conv = co_ref[...].astype(f32)
     mean = column(stat_total(0), spread) / CH
@@ -459,30 +538,12 @@
     rstd_ref[...] = rstd
     coef_ref[...] = norm_sig * (1.0 + norm_pre * (1.0 - norm_sig)) * gain_ref[...]
 
-    for g in range(NG):
-        span = home_ref.at[pl.ds(1, GB - 1)] if g == 0 else home_ref.at[pl.ds(g * GB, GB)]
-        remote(span, span, bsend.at[g], brecv.at[g], peer_at(1), x).wait_recv()
-
-    @pl.loop(0, NSP)
-    def _(e):
-        for j in range(2):
-            for rt in range(2):
-                for ct in range(4):
-                    flat_ref[at(e * 32 + rt * 16, 16, 16), pl.ds(j * QW + ct * 128, 128)] = (
-                        home_ref[e, j, rt * 4 + ct]
-                    )
-            flatr_ref[at(e * 16, 16, 16), pl.ds(j * 128, 128)] = home_ref[e, j, 8]
-
-    rem_group = (iota((512, 1), 0) % 16) // 4
-    sums = []
-    for j in range(2):
-        main = dot(ohm_ref[...], flat_ref[:, j * QW : (j + 1) * QW], 0, 0)
-        rems = flatr_ref[:, j * 128 : (j + 1) * 128].astype(f32)
-        tails = [jnp.where(rem_group == cg, rems, 0.0).astype(bf16) for cg in range(4)]
-        sums.append(main + dot(ohr_ref[...], jnp.concatenate(tails, axis=1), 0, 0))
-    exo_ref[0] = sums[0][:, 256:].astype(bf16)
-    exo_ref[1] = sums[1][:, :256].astype(bf16)
-
+    @pl.loop(0, NG - 1)
+    def _(g):
+        home_wait(g)
+        combine(g)
+
+    home_wait(NG - 1)
     def exchange(side):
         return remote(
             exo_ref.at[side],
@@ -493,21 +554,27 @@
             to_left_or_right(side),
         )
 
-    for side in range(2):
-        exchange(side).start()
+    combine(NG - 1, (1,))
+    exo_ref[1] = sum_ref[:, QW : QW + 256].astype(bf16)
+    exchange(1).start()
+    combine(NG - 1, (0,))
+    exo_ref[0] = sum_ref[:, 256:QW].astype(bf16)
+    exchange(0).start()
+    weight_grads(1)
+    weight_grads(2)
     for side in range(2):
         exchange(side).wait_recv()
     cot0 = c_ref[:, at(quarter(0) * QW, 256, 256)].astype(f32)
     cot1 = c_ref[:, at(quarter(1) * QW + 256, 256, 256)].astype(f32)
-    ag_ref[0, 0] = (cot0 + (sums[0][:, :256] + exi_ref[1].astype(f32))).astype(bf16)
-    ag_ref[0, 1] = (cot1 + (sums[1][:, 256:] + exi_ref[0].astype(f32))).astype(bf16)
-
-    def gather(side):
+    ag_ref[0, 0] = (cot0 + (sum_ref[:, :256] + exi_ref[1].astype(f32))).astype(bf16)
+    ag_ref[0, 1] = (cot1 + (sum_ref[:, QW + 256 :] + exi_ref[0].astype(f32))).astype(bf16)
+
+    def gather(side, part):
         return remote(
-            ag_ref.at[0],
-            ag_ref.at[3 if side else 1],
-            asend.at[side],
-            arecv.at[side],
+            ag_ref.at[0, part],
+            ag_ref.at[3 if side else 1, part],
+            asend.at[side, part],
+            arecv.at[side, part],
             me,
             to_left_or_right(side),
         )
@@ -516,64 +583,74 @@
         return remote(
             ag_ref.at[3 if side else 1, 1 - side],
             ag_ref.at[2, 1 - side],
-            asend.at[2 + side],
-            arecv.at[2 + side],
+            asend.at[2, side],
+            arecv.at[2, side],
             me,
             to_left_or_right(side),
         )
 
-    def place(o):
-        resid_ref[:, at(quarter(o) * QW, 256, 256)] = ag_ref[o, 0]
-        resid_ref[:, at(quarter(o + 1) * QW + 256, 256, 256)] = ag_ref[o, 1]
+    def place(o, part):
+        cols = at(quarter(o + part) * QW + part * 256, 256, 256)
+        resid_ref[:, cols] = ag_ref[o, part]
+        return dot(ag_ref[o, part], ow_ref[:, cols], 1, 1)
+
+    def owg_copy(peer):
+        return remote(pso_ref.at[peer], psi_ref.at[me], psend.at[0], precv.at[0], peer, x)
+
+    def project(o, part):
+        term = dot(ag_ref[o, part], act_ref[...], 0, 0).astype(bf16)
+        for i in range(4):
+            peer = quarter(o + part) * 8 + part * 4 + i
+            for rt in range(4):
+                for ct in range(2):
+                    pso_ref[peer, rt * 2 + ct] = term[
+                        i * OW + rt * 16 : i * OW + rt * 16 + 16, ct * 128 : ct * 128 + 128
+                    ]
+
+        for i in range(4):
+            peer = quarter(o + part) * 8 + part * 4 + (i + me) % 4
+
+            @pl.when(peer == me)
+            def _():
+                psi_ref[me] = pso_ref[me]
+
+            @pl.when(peer != me)
+            def _():
+                owg_copy(peer).start()
 
     for side in range(2):
-        gather(side).start()
-    place(0)
+        gather(side, 1 - side).start()
     for side in range(2):
-        gather(side).wait_recv()
+        gather(side, side).start()
+    mix_grad = place(0, 0) + place(0, 1)
+    project(0, 0)
+    project(0, 1)
+    weight_grads(3)
+    for store in stores[:3]:
+        store.start()
+    for side in range(2):
+        gather(side, 1 - side).wait_recv()
         gather_far(side).start()
-    place(1)
-    place(3)
+    mix_grad = mix_grad + place(1, 1) + place(3, 0)
+    project(1, 1)
+    project(3, 0)
+    for side in range(2):
+        gather(side, side).wait_recv()
+    mix_grad = mix_grad + place(1, 0) + place(3, 1)
+    project(1, 0)
+    project(3, 1)
     for side in range(2):
         gather_far(side).wait_recv()
-    place(2)
+    mix_grad = mix_grad + place(2, 0) + place(2, 1)
     stores[3].start()
 
-    mix_grad = dot(resid_ref[...], ow_ref[...], 1, 1)
     norm_grad = mix_grad * coef_ref[...]
     sum_rows = exact_dot(ones, norm_grad, 1, 1)
     dot_rows = exact_dot(ones, norm_grad * normed_ref[...], 1, 1)
     stat_start(2, jnp.where(iota((8, ROWS), 0) == 0, sum_rows, dot_rows))
 
-    def owg_copy(k, peer):
-        return remote(pso_ref.at[k], psi_ref.at[k], psend.at[0], precv.at[0], peer, x)
-
-    @pl.loop(0, 4)
-    def _(g):
-        cols = at(g * QW, QW, QW)
-        term = dot(resid_ref[:, cols], act_ref[...], 0, 0).astype(bf16)
-        for i in range(8):
-            for rt in range(4):
-                for ct in range(2):
-                    flat_ref[
-                        at((g % 2) * 512 + i * OW + rt * 16, 16, 16),
-                        at((g // 2) * 256 + ct * 128, 128, 128),
-                    ] = term[i * OW + rt * 16 : i * OW + rt * 16 + 16, ct * 128 : ct * 128 + 128]
-
-    @pl.loop(0, NSP)
-    def _(k):
-        peer = peer_at(k)
-        for rt in range(4):
-            for ct in range(2):
-                pso_ref[k, rt * 2 + ct] = flat_ref[
-                    at((peer % 16) * OW + rt * 16, 16, 16),
-                    at((peer // 16) * 256 + ct * 128, 128, 128),
-                ]
-
-        @pl.when(k > 0)
-        def _():
-            owg_copy(k, peer).start()
-
+    project(2, 0)
+    project(2, 1)
     totals = stat_total(2)
     conv_grad = rstd_ref[...] * (
         norm_grad
@@ -615,11 +692,11 @@
 
     convolve(ROWS - 32, 32)
 
-    whole = psi_ref.at[pl.ds(1, NSP - 1)]
+    whole = psi_ref.at[pl.ds(0, NSP - 1)]
     remote(whole, whole, psend.at[0], precv.at[0], me, right).wait_recv()
     for rt in range(4):
         for ct in range(2):
-            total = pso_ref[0, rt * 2 + ct].astype(f32)
+            total = psi_ref[0, rt * 2 + ct].astype(f32)
             for k in range(1, NSP):
                 total = total + psi_ref[k, rt * 2 + ct].astype(f32)
             owg_ref[rt * 16 : rt * 16 + 16, ct * 128 : ct * 128 + 128] = total
@@ -634,20 +711,29 @@
         remote(sent, sent, ssend.at[n], srecv.at[n], me, right).wait_send()
     for side in range(2):
         exchange(side).wait_send()
-        gather(side).wait_send()
+        gather(side, 0).wait_send()
+        gather(side, 1).wait_send()
         gather_far(side).wait_send()
-        sent = got_ref.at[:, :, side]
+        sent = got_ref.at[:, pl.ds(0, NSP - WHOLE), side]
         remote(sent, sent, xfsend.at[side], xfrecv.at[0, side], me, right).wait_send()
         for g in range(NG):
             pair_copy(g, side).wait_send()
     for t in range(2):
         sent = send_ref.at[t, pl.ds(0, NSP - 1)]
         remote(sent, sent, fsend.at[t], frecv.at[t, 0], me, right).wait_send()
+    sent = more_ref.at[:, pl.ds(0, WHOLE - 1)]
+    remote(sent, sent, msend.at[0], mrecv.at[0, 0], me, right).wait_send()
     for g in range(NG):
         sent = back_ref.at[pl.ds(0, GB - 1 if g == 0 else GB)]
         remote(sent, sent, bsend.at[g], brecv.at[g], me, right).wait_send()
     for store in stores:
         store.wait()
+
+
+def widen_kernel(*refs):
+    half = len(refs) // 2
+    for src, dst in zip(refs[:half], refs[half:]):
+        dst[...] = src[...].astype(dst.dtype)
 
 
 def on_device(
@@ -699,9 +785,9 @@
             pltpu.VMEM((ROWS, D), bf16),
             pltpu.VMEM((NSP, ROWS), jnp.int32),
             pltpu.VMEM((NSP, ROWS), f32),
-            pltpu.VMEM((1024, ROWS), bf16),
-            pltpu.VMEM((512, ROWS), bf16),
+            pltpu.VMEM((NG * GO, ROWS), bf16),
             pltpu.VMEM((2, NSP, 2, NT, 16, 128), bf16),
+            pltpu.VMEM((2, WHOLE, 2, NT, 16, 128), bf16),
             pltpu.VMEM((2, NSP, 4, NT, 16, 128), bf16),
             pltpu.VMEM((2, NSP * 36, D), bf16),
             pltpu.VMEM((3, NSP * 36, FG), bf16),
@@ -709,8 +795,7 @@
             pltpu.VMEM((2, NSP, NT, 16, 128), bf16),
             pltpu.VMEM((NSP, 2, NT, 16, 128), bf16),
             pltpu.VMEM((NSP, 2, NT, 16, 128), bf16),
-            pltpu.VMEM((1024, 1024), bf16),
-            pltpu.VMEM((512, 256), bf16),
+            pltpu.VMEM((ROWS, 2 * QW), f32),
             pltpu.VMEM((2, ROWS, 256), bf16),
             pltpu.VMEM((2, ROWS, 256), bf16),
             pltpu.VMEM((4, 2, ROWS, 256), bf16),
@@ -727,6 +812,8 @@
             dma((4,)),
             dma((2,)),
             dma((2, NSP)),
+            dma((1,)),
+            dma((2, WHOLE)),
             dma((2,)),
             dma((NG, 2)),
             dma((NG, 2)),
@@ -735,8 +822,8 @@
             dma((NG,)),
             dma((2,)),
             dma((2,)),
-            dma((4,)),
-            dma((4,)),
+            dma((3, 2)),
+            dma((3, 2)),
             dma((3,)),
             dma((3,)),
             dma((1,)),
@@ -764,10 +851,25 @@
         norm_gain[None, :],
         norm_bias[None, :],
     )
+    steps = 4
+
+    def block(rows, cols):
+        return pl.BlockSpec((rows // steps, cols), lambda n: (n, 0))
+
+    sizes = [(D, FG), (D, FG), (FG, D), (ROWS, D), (OW, FG), (ROWS, FG), (ROWS, FG)]
+    types = [f32, f32, f32, bf16, f32, bf16, bf16]
+    gate_grad, up_grad, down_grad, resid_grad, projected, value_grad, gate_in_grad = pl.pallas_call(
+        widen_kernel,
+        grid=(steps,),
+        out_shape=tuple(shape(size, kind) for size, kind in zip(sizes, types)),
+        in_specs=[block(*size) for size in sizes],
+        out_specs=tuple(block(*size) for size in sizes),
+        name="widen",
+    )(gate_grad, up_grad, down_grad, resid_grad, projected, value_grad, gate_in_grad)
     return (
-        gate_grad[None].astype(f32),
-        up_grad[None].astype(f32),
-        down_grad[None].astype(f32),
+        gate_grad[None],
+        up_grad[None],
+        down_grad[None],
         resid_grad,
         projected.T,
         value_grad,

time: 161 us -> 147 us (0.913)
  other arithmetic: 5.53 us -> 0 us
  Pallas kernels: 150 us -> 146 us
  local copies, waits for them, and re-layouts: 3.5 us -> 0 us
    pallas_call x1, Pallas kernels: 150 us -> 140 us  [on_device(): pl.pallas_call(layer_kernel, out_shape=(shape((D, FG), bf16), shape((D, F...]
    pallas_call x0 -> x1, Pallas kernels: none -> 6.04 us  [on_device(): pl.pallas_call(widen_kernel, grid=(steps,), out_shape=tuple((shape(size,...]
    convert_element_type x2 -> x0, other arithmetic: 5.53 us -> none  [the longest x1 3.97 us: on_device(): up_grad[None].astype(f32)]
    unnamed x14 -> x0, local copies, waits for them, and re-layouts: 3.5 us -> none
where the time goes in v3:
time: 147 us
  Pallas kernels  146 us (99%)
    pallas_call x1, Pallas kernels, on_device(): pl.pallas_call(layer_kernel, out_shape=(shape((D, FG), bf16), shape((D, F...  140 us
    pallas_call x1, Pallas kernels, on_device(): pl.pallas_call(widen_kernel, grid=(steps,), out_shape=tuple((shape(size,...  6.04 us

profile of v3, /device:TPU:1, one launch (start us, length us, event | category | flops | bytes accessed | tf_op | source)
XLA Modules:
  0.0 146.8 jit_solution(6301610722443772945)
XLA Ops:
  0.6 140.0 %layer.1 = (bf16[2048,256]{1,0:T(8,128)(2,1)}, bf16[2048,256]{1,0:T(8,128)(2,1)}, bf16[256,2048]{1,0:T(8,128)(2,1)}, bf16[384,2048]{1,0:T(8,128)(2,1)}, f32[64,2...) custom-call(bf16[384,2048]{1,0:T(8,128)(2,1)} %x_hbm.1, bf16[384,2048]{1,0:T(8,128)(2,1)} %c_hbm.1, ...), custom_call_target="tpu_custom_call" | custom-call | tf_op jit(solution)/shard_map/layer/pallas_call | solution.py:759
  140.6 6.0 %widen.1 = (f32[2048,256]{1,0:T(8,128)}, f32[2048,256]{1,0:T(8,128)}, f32[256,2048]{1,0:T(8,128)}, bf16[384,2048]{1,0:T(8,128)(2,1)}, f32[64,256]{1,0:T(8,128)},...) custom-call(bf16[2048,256]{1,0:T(8,128)(2,1)} %get-tuple-element.21.refs_0_, ...), custom_call_target="tpu_custom_call" | custom-call | tf_op jit(solution)/shard_map/widen/pallas_call | solution.py:861

commit v4 on v3

--- a/solution.py
+++ b/solution.py
@@ -37,6 +37,16 @@
 
 def exact_dot(a, b, ca=1, cb=0):
     return dot(a, b, ca, cb, lax.Precision.HIGHEST)
+
+
+def split(a):
+    high = a.astype(bf16)
+    return high, (a - high.astype(f32)).astype(bf16)
+
+
+def row_sums(a):
+    high, low = split(a)
+    return dot(jnp.ones((8, 2 * FG), bf16), jnp.concatenate([high, low], axis=1), 1, 1)
 
 
 def iota(shape, dim):
@@ -107,6 +117,7 @@
     halo_ref,
     pso_ref,
     psi_ref,
+    pin_ref,
     insem,
     outsem,
     fsend,
@@ -129,6 +140,8 @@
     hrecv,
     psend,
     precv,
+    dsend,
+    drecv,
 ):
     me = lax.axis_index("sp")
     x = lax.axis_index("tp")
@@ -316,7 +329,10 @@
         return (stat_ref[n, 0] + stat_ref[n, 1]) + (stat_ref[n, 2] + stat_ref[n, 3])
 
     def column(row_form, pick):
-        one = exact_dot(row_form, pick, 0, 0)
+        high, low = split(row_form)
+        low2 = (row_form - high.astype(f32) - low.astype(f32)).astype(bf16)
+        terms = jnp.concatenate([high, low, low2, jnp.zeros_like(high)], axis=0)
+        one = dot(terms, jnp.concatenate([pick] * 4, axis=0).astype(bf16), 0, 0)
         return jnp.concatenate([one, one], axis=1)
 
 
@@ -501,6 +517,25 @@
                 load.wait()
             stat_start(0, exact_dot(ones, co_ref[...].astype(f32), 1, 1))
 
+        @pl.when(step == 2)
+        def _():
+            mean = column(stat_total(0), spread) / CH
+            centred = co_ref[...].astype(f32) - mean
+            normed_ref[...] = centred
+            stat_start(1, exact_dot(ones, centred * centred, 1, 1))
+
+        @pl.when(step == 4)
+        def _():
+            var = column(stat_total(1), spread) / CH
+            rstd = lax.rsqrt(var + norm_eps)
+            normed = normed_ref[...] * rstd
+            norm_pre = normed * gain_ref[...] + bias_ref[...]
+            norm_sig = jax.nn.sigmoid(norm_pre)
+            act_ref[...] = (norm_pre * norm_sig).astype(bf16)
+            normed_ref[...] = normed
+            rstd_ref[...] = rstd
+            coef_ref[...] = norm_sig * (1.0 + norm_pre * (1.0 - norm_sig)) * gain_ref[...]
+
         @pl.when((step > 0) & (step < NG + 1))
         def _():
             experts(step - 1)
@@ -523,20 +558,6 @@
         )
     ]
     weight_grads(0)
-
-    conv = co_ref[...].astype(f32)
-    mean = column(stat_total(0), spread) / CH
-    centred = conv - mean
-    stat_start(1, exact_dot(ones, centred * centred, 1, 1))
-    var = column(stat_total(1), spread) / CH
-    rstd = lax.rsqrt(var + norm_eps)
-    normed = centred * rstd
-    norm_pre = normed * gain_ref[...] + bias_ref[...]
-    norm_sig = jax.nn.sigmoid(norm_pre)
-    act_ref[...] = (norm_pre * norm_sig).astype(bf16)
-    normed_ref[...] = normed
-    rstd_ref[...] = rstd
-    coef_ref[...] = norm_sig * (1.0 + norm_pre * (1.0 - norm_sig)) * gain_ref[...]
 
     @pl.loop(0, NG - 1)
     def _(g):
@@ -594,29 +615,51 @@
         resid_ref[:, cols] = ag_ref[o, part]
         return dot(ag_ref[o, part], ow_ref[:, cols], 1, 1)
 
+    def owner(o, part, i):
+        return quarter(o + part) * 8 + part * 4 + i
+
+    def partner_copy(o, peer):
+        return remote(
+            pso_ref.at[peer],
+            pin_ref.at[peer // 2],
+            dsend.at[0],
+            drecv.at[o],
+            (me // 2) * 2 + 1 - core,
+            x,
+        )
+
     def owg_copy(peer):
-        return remote(pso_ref.at[peer], psi_ref.at[me], psend.at[0], precv.at[0], peer, x)
+        return remote(
+            pso_ref.at[peer], psi_ref.at[me // 2], psend.at[0], precv.at[0], peer, x
+        )
 
     def project(o, part):
         term = dot(ag_ref[o, part], act_ref[...], 0, 0).astype(bf16)
         for i in range(4):
-            peer = quarter(o + part) * 8 + part * 4 + i
             for rt in range(4):
                 for ct in range(2):
-                    pso_ref[peer, rt * 2 + ct] = term[
+                    pso_ref[owner(o, part, i), rt * 2 + ct] = term[
                         i * OW + rt * 16 : i * OW + rt * 16 + 16, ct * 128 : ct * 128 + 128
                     ]
-
-        for i in range(4):
-            peer = quarter(o + part) * 8 + part * 4 + (i + me) % 4
-
-            @pl.when(peer == me)
-            def _():
-                psi_ref[me] = pso_ref[me]
-
-            @pl.when(peer != me)
-            def _():
-                owg_copy(peer).start()
+        for i in range(2):
+            partner_copy(o, owner(o, part, 2 * i + 1 - core)).start()
+
+    def relay(o):
+        four = pin_ref.at[pl.ds(0, 4)]
+        remote(four, four, dsend.at[0], drecv.at[o], me, right).wait_recv()
+        for part in range(2):
+            for i in range(2):
+                peer = owner(o, part, 2 * i + core)
+                both = pso_ref[peer].astype(f32) + pin_ref[peer // 2].astype(f32)
+                pso_ref[peer] = both.astype(bf16)
+
+                @pl.when(peer == me)
+                def _():
+                    psi_ref[me // 2] = pso_ref[me]
+
+                @pl.when(peer != me)
+                def _():
+                    owg_copy(peer).start()
 
     for side in range(2):
         gather(side, 1 - side).start()
@@ -632,6 +675,7 @@
         gather(side, 1 - side).wait_recv()
         gather_far(side).start()
     mix_grad = mix_grad + place(1, 1) + place(3, 0)
+    relay(0)
     project(1, 1)
     project(3, 0)
     for side in range(2):
@@ -639,18 +683,21 @@
     mix_grad = mix_grad + place(1, 0) + place(3, 1)
     project(1, 0)
     project(3, 1)
+    relay(1)
+    relay(3)
     for side in range(2):
         gather_far(side).wait_recv()
     mix_grad = mix_grad + place(2, 0) + place(2, 1)
     stores[3].start()
 
     norm_grad = mix_grad * coef_ref[...]
-    sum_rows = exact_dot(ones, norm_grad, 1, 1)
-    dot_rows = exact_dot(ones, norm_grad * normed_ref[...], 1, 1)
+    sum_rows = row_sums(norm_grad)
+    dot_rows = row_sums(norm_grad * normed_ref[...])
     stat_start(2, jnp.where(iota((8, ROWS), 0) == 0, sum_rows, dot_rows))
 
     project(2, 0)
     project(2, 1)
+    relay(2)
     totals = stat_total(2)
     conv_grad = rstd_ref[...] * (
         norm_grad
@@ -692,12 +739,12 @@
 
     convolve(ROWS - 32, 32)
 
-    whole = psi_ref.at[pl.ds(0, NSP - 1)]
+    whole = psi_ref.at[pl.ds(0, NSP // 2 - 1)]
     remote(whole, whole, psend.at[0], precv.at[0], me, right).wait_recv()
     for rt in range(4):
         for ct in range(2):
             total = psi_ref[0, rt * 2 + ct].astype(f32)
-            for k in range(1, NSP):
+            for k in range(1, NSP // 2):
                 total = total + psi_ref[k, rt * 2 + ct].astype(f32)
             owg_ref[rt * 16 : rt * 16 + 16, ct * 128 : ct * 128 + 128] = total
 
@@ -706,6 +753,7 @@
         halo_copy(me - 1).wait_send()
 
     remote(whole, whole, psend.at[0], precv.at[0], me, right).wait_send()
+    remote(pin_ref, pin_ref, dsend.at[0], drecv.at[0], me, right).wait_send()
     for n in range(3):
         sent = stat_ref.at[n, pl.ds(1, NTP - 1)]
         remote(sent, sent, ssend.at[n], srecv.at[n], me, right).wait_send()
@@ -807,7 +855,8 @@
             pltpu.VMEM((ROWS + 32, FG), f32),
             pltpu.VMEM((32, FG), f32),
             pltpu.VMEM((NSP, 8, 16, 128), bf16),
-            pltpu.VMEM((NSP, 8, 16, 128), bf16),
+            pltpu.VMEM((NSP // 2, 8, 16, 128), bf16),
+            pltpu.VMEM((NSP // 2, 8, 16, 128), bf16),
             dma((9,)),
             dma((4,)),
             dma((2,)),
@@ -830,6 +879,8 @@
             dma((1,)),
             dma((1,)),
             dma((1,)),
+            dma((1,)),
+            dma((4,)),
         ],
         compiler_params=pltpu.CompilerParams(
             collective_id=0, has_side_effects=True, vmem_limit_bytes=67000000
@@ -851,7 +902,7 @@
         norm_gain[None, :],
         norm_bias[None, :],
     )
-    steps = 4
+    steps = 2
 
     def block(rows, cols):
         return pl.BlockSpec((rows // steps, cols), lambda n: (n, 0))

time: 147 us -> 144 us (0.980)
  Pallas kernels: 146 us -> 142 us
    pallas_call x1, Pallas kernels: 140 us -> 137 us  [on_device(): pl.pallas_call(layer_kernel, out_shape=(shape((D, FG), bf16), shape((D, F...]
where the time goes in v4:
time: 144 us; the launch traced here: 143 us
  Pallas kernels  142 us (99%)
    pallas_call x1, Pallas kernels, on_device(): pl.pallas_call(layer_kernel, out_shape=(shape((D, FG), bf16), shape((D, F...  137 us
    pallas_call x1, Pallas kernels, on_device(): pl.pallas_call(widen_kernel, grid=(steps,), out_shape=tuple((shape(size,...  5.22 us

profile of v4, /device:TPU:1, one launch (start us, length us, event | category | flops | bytes accessed | tf_op | source)
XLA Modules:
  0.0 143.3 jit_solution(8569899451142511895)
XLA Ops:
  0.6 137.2 %layer.1 = (bf16[2048,256]{1,0:T(8,128)(2,1)}, bf16[2048,256]{1,0:T(8,128)(2,1)}, bf16[256,2048]{1,0:T(8,128)(2,1)}, bf16[384,2048]{1,0:T(8,128)(2,1)}, f32[64,2...) custom-call(bf16[384,2048]{1,0:T(8,128)(2,1)} %x_hbm.1, bf16[384,2048]{1,0:T(8,128)(2,1)} %c_hbm.1, ...), custom_call_target="tpu_custom_call" | custom-call | tf_op jit(solution)/shard_map/layer/pallas_call | solution.py:807
  137.9 5.2 %widen.1 = (f32[2048,256]{1,0:T(8,128)}, f32[2048,256]{1,0:T(8,128)}, f32[256,2048]{1,0:T(8,128)}, bf16[384,2048]{1,0:T(8,128)(2,1)}, f32[64,256]{1,0:T(8,128)},...) custom-call(bf16[2048,256]{1,0:T(8,128)(2,1)} %get-tuple-element.21.refs_0_, ...), custom_call_target="tpu_custom_call" | custom-call | tf_op jit(solution)/shard_map/widen/pallas_call | solution.py:912

commit v5 on v4

--- a/solution.py
+++ b/solution.py
@@ -118,6 +118,7 @@
     pso_ref,
     psi_ref,
     pin_ref,
+    gates_ref,
     insem,
     outsem,
     fsend,
@@ -517,6 +518,12 @@
                 load.wait()
             stat_start(0, exact_dot(ones, co_ref[...].astype(f32), 1, 1))
 
+        @pl.when(step == 5)
+        def _():
+            gate_sig = jax.nn.sigmoid(cg_ref[...].astype(f32))
+            gates_ref[0] = gate_sig
+            gates_ref[1] = cv_ref[...].astype(f32) * gate_sig * (1.0 - gate_sig)
+
         @pl.when(step == 2)
         def _():
             mean = column(stat_total(0), spread) / CH
@@ -719,11 +726,8 @@
             begin = start + KW - 1 - lag
             glu = glu + taps_ref[lag : lag + 1, :] * ext_ref[begin : begin + rows, :]
         span = pl.ds(start, rows)
-        gate_sig = jax.nn.sigmoid(cg_ref[span, :].astype(f32))
-        value_ref[span, :] = (glu * gate_sig).astype(bf16)
-        gatein_ref[span, :] = (
-            glu * cv_ref[span, :].astype(f32) * gate_sig * (1.0 - gate_sig)
-        ).astype(bf16)
+        value_ref[span, :] = (glu * gates_ref[0, span, :]).astype(bf16)
+        gatein_ref[span, :] = (glu * gates_ref[1, span, :]).astype(bf16)
 
     for start in range(0, ROWS - 32, 32):
         convolve(start, 32)
@@ -857,6 +861,7 @@
             pltpu.VMEM((NSP, 8, 16, 128), bf16),
             pltpu.VMEM((NSP // 2, 8, 16, 128), bf16),
             pltpu.VMEM((NSP // 2, 8, 16, 128), bf16),
+            pltpu.VMEM((2, ROWS, FG), f32),
             dma((9,)),
             dma((4,)),
             dma((2,)),

time: 144 us -> 144 us (level)
  no operation moved by 1% of the time
where the time goes in v5:
time: 144 us; the launch traced here: 143 us
  Pallas kernels  142 us (99%)
    pallas_call x1, Pallas kernels, on_device(): pl.pallas_call(layer_kernel, out_shape=(shape((D, FG), bf16), shape((D, F...  137 us
    pallas_call x1, Pallas kernels, on_device(): pl.pallas_call(widen_kernel, grid=(steps,), out_shape=tuple((shape(size,...  5.22 us

profile of v5, /device:TPU:1, one launch (start us, length us, event | category | flops | bytes accessed | tf_op | source)
XLA Modules:
  0.0 143.1 jit_solution(10253057851330949561)
XLA Ops:
  0.6 137.1 %layer.1 = (bf16[2048,256]{1,0:T(8,128)(2,1)}, bf16[2048,256]{1,0:T(8,128)(2,1)}, bf16[256,2048]{1,0:T(8,128)(2,1)}, bf16[384,2048]{1,0:T(8,128)(2,1)}, f32[64,2...) custom-call(bf16[384,2048]{1,0:T(8,128)(2,1)} %x_hbm.1, bf16[384,2048]{1,0:T(8,128)(2,1)} %c_hbm.1, ...), custom_call_target="tpu_custom_call" | custom-call | tf_op jit(solution)/shard_map/layer/pallas_call | solution.py:811
  137.8 5.2 %widen.1 = (f32[2048,256]{1,0:T(8,128)}, f32[2048,256]{1,0:T(8,128)}, f32[256,2048]{1,0:T(8,128)}, bf16[384,2048]{1,0:T(8,128)(2,1)}, f32[64,256]{1,0:T(8,128)},...) custom-call(bf16[2048,256]{1,0:T(8,128)(2,1)} %get-tuple-element.21.refs_0_, ...), custom_call_target="tpu_custom_call" | custom-call | tf_op jit(solution)/shard_map/widen/pallas_call | solution.py:917
